TPU v7x, 512 devices: a whole 4x4x16 slice. The times are simulated.
512 devices in a mesh: fs: 64 (over z, y), tp: 8 (over x, core).
Axes of the slice: x: 4, y: 4, z: 16, core: 2. Of those that a mesh axis runs over, the one named last changes fastest.
Arguments:
- tokens: bfloat16 [49152, 2048], P('fs'), may hold values from -6 to 6
- norm_gain: float32 [2048], replicated, may hold values from 0.1 to 1.9
- gate_weight: float32 [2048, 5120], P('fs', 'tp'), may hold values from -0.125 to 0.125
- value_weight: float32 [2048, 5120], P('fs', 'tp'), may hold values from -0.125 to 0.125
- gate_scale: float32 [5120], P('tp'), may hold values from 0.3 to 3
- value_scale: float32 [5120], P('tp'), may hold values from 0.3 to 3
- gate_kernel: float32 [3, 5120], P(None, 'tp'), may hold values from -3.5 to 3.5
- value_kernel: float32 [3, 5120], P(None, 'tp'), may hold values from -3.5 to 3.5
- gate_bias: float32 [5120], P('tp'), may hold values from -3 to 3
- value_bias: float32 [5120], P('tp'), may hold values from -3 to 3
- down_weight: float32 [5120, 2048], P('tp', 'fs'), may hold values from -0.078125 to 0.078125
- down_scale: float32 [2048], P('tp'), may hold values from 0.3 to 3
Outputs:
- mixed: bfloat16 [49152, 2048], P('fs', 'tp')
All inputs are finite; a program needn't handle non-finite values.
Results may differ from a plain program's by a relative error of at most 0.014.
Values may be sent and summed in bfloat16 or wider, within the bound.
No kernel may reach another device: no remote copies, remote signals or barrier semaphores. Data moves between devices by JAX's collectives and lax.ppermute only.
A program may use at most 64 MiB of HBM per device.

v0:
```python
import jax
import jax.numpy as jnp
from jax import lax
from jax.sharding import PartitionSpec as P

epsilon = 1e-06


def gather_turned(arrays, axis, dims):
    turned = [jnp.moveaxis(a, dim, 0) for a, dim in zip(arrays, dims)]
    both = jnp.concatenate([t.reshape(len(t), -1) for t in turned], axis=1)
    result, at, done = (lax.all_gather(both, axis, axis=0, tiled=True), 0, [])
    for t, dim in zip(turned, dims):
        section = result[:, at : at + t[0].size].reshape(-1, *t.shape[1:])
        done.append(jnp.moveaxis(section, 0, dim))
        at += t[0].size
    return tuple(done)


def from_behind(value, axis, steps):
    count = lax.axis_size(axis)
    leading, last = (max(0, -steps), min(count, count - steps))
    return lax.ppermute(value, axis, [(source, source + steps) for source in range(leading, last)])


def normalize(tokens, norm_gain):
    values = tokens.astype(jnp.float32)
    scaled = values * lax.rsqrt(jnp.mean(values * values, axis=1, keepdims=True) + epsilon)
    return (scaled * norm_gain[None, :]).astype(jnp.bfloat16)


def causal_mix(current, previous, kernel, tap_bias):
    row_count = current.shape[0]
    joined = jnp.concatenate([previous, current], axis=0).astype(jnp.float32)
    summed_taps = tap_bias[None, :] + kernel[2][None, :] * joined[2:]
    for back_by in (1, 2):
        summed_taps = (
            summed_taps
            + kernel[2 - back_by][None, :] * joined[2 - back_by : 2 - back_by + row_count]
        )
    return summed_taps


def body(
    tokens,
    norm_gain,
    gate_weight,
    value_weight,
    gate_scale,
    value_scale,
    gate_kernel,
    value_kernel,
    gate_bias,
    value_bias,
    down_weight,
    down_scale,
):
    normed = normalize(tokens, norm_gain)
    gate_low = gate_weight.astype(jnp.bfloat16)
    value_low = value_weight.astype(jnp.bfloat16)
    down_low = down_weight.astype(jnp.bfloat16)
    row_count = normed.shape[0]
    gate_full, value_full, down_full = gather_turned(
        (gate_low, value_low, down_low), "fs", (0, 0, 1)
    )
    gate_raw = jnp.dot(normed, gate_full, preferred_element_type=jnp.float32)
    value_raw = jnp.dot(normed, value_full, preferred_element_type=jnp.float32)
    gate_pre = (gate_raw * gate_scale[None, :]).astype(jnp.bfloat16)
    value_pre = (value_raw * value_scale[None, :]).astype(jnp.bfloat16)
    previous_gate, previous_value = from_behind(
        (gate_pre[row_count - 2 :], value_pre[row_count - 2 :]), "fs", 1
    )
    gate_conv = causal_mix(gate_pre, previous_gate, gate_kernel, gate_bias)
    value_conv = causal_mix(value_pre, previous_value, value_kernel, value_bias)
    hidden = (jax.nn.gelu(gate_conv, approximate=True) * value_conv).astype(jnp.bfloat16)
    partial_terms = jnp.dot(hidden, down_full, preferred_element_type=jnp.float32)
    summed = lax.psum_scatter(
        partial_terms.astype(jnp.bfloat16), "tp", scatter_dimension=1, tiled=True
    ).astype(jnp.float32)
    return (summed * down_scale[None, :]).astype(jnp.bfloat16)


def solution(mesh):
    return jax.shard_map(
        body,
        mesh=mesh,
        in_specs=(
            P("fs", None),
            P(),
            P("fs", "tp"),
            P("fs", "tp"),
            P("tp"),
            P("tp"),
            P(None, "tp"),
            P(None, "tp"),
            P("tp"),
            P("tp"),
            P("tp", "fs"),
            P("tp"),
        ),
        out_specs=P("fs", "tp"),
        check_vma=False,
    )
```

profile of v0, /device:TPU:1, one launch (start us, length us, event | category | flops | bytes accessed | tf_op | source)
XLA Modules:
  0.0 238.9 jit_solution(17167941775275477167)
XLA Ops:
  6.5 0.0 copy-start
  6.5 0.0 copy-start.3
  6.5 0.0 copy-start.4
  6.5 0.0 all-gather.2.cloned.1.call-start
  6.5 1.0 convert_element_type.41
  7.6 0.9 convert_element_type.42
  8.5 0.9 convert_bitcast_fusion
  9.4 0.7 pad_maximum_fusion
  10.0 0.0 all-gather.2.cloned.1.call-update
  10.1 0.0 reduce-scatter.2.cloned.1.call-start
  10.1 0.9 slice_reduce_fusion.2
  11.0 2.6 %fusion = f32[768]{0:T(1024)S(1)} fusion(bf16[768,2048]{1,0:T(8,128)(2,1)} %param.12), kind=kLoop, calls=%fused_computation.2 | loop fusion | flops 4717824 | bytes 3148800 | tf_op jit(solution)/shard_map/reduce_sum | solution.py:28
  13.6 0.0 copy-start.5
  13.6 148.7 %all-gather.2.cloned.1.call-done = bf16[2048,1920]{1,0:T(8,128)(2,1)} async-done(((bf16[32,1920]{1,0:T(8,128)(2,1)}), bf16[2048,1920]{1,0:T(8,128)(2,1)}) %all-gather.2.cloned.1.call-update) | async-done | bytes 7864336 | tf_op jit(solution)/shard_map/all_gather | solution.py:12
  162.3 0.0 copy-done
  162.3 0.0 copy-done.3
  162.3 0.0 copy-done.4
  162.3 0.0 copy-start.2
  162.3 4.5 %multiply_convert_fusion.1 = bf16[768,640]{1,0:T(8,128)(2,1)S(1)} fusion(bf16[2048,1920]{1,0:T(8,128)(2,1)} %all-gather.2.cloned.1.call-done, f32[640]{0:T(1024)S(1)} %copy-done.4, bf16[768,2048]{1,0:T(8,128)(2,1)S(1)} %copy-done, f32[2048]{0:T(1024)S(1)} %copy-done.3, f32[768]{0:T(1024)S(1)} %add_rsqrt_fusion), kind=kOutput, calls=%fused_computation.34 | convolution fusion | flops 2020540416 | bytes 6764032 | tf_op jit(solution)/shard_map/dot_general | solution.py:66
  166.9 1.8 collective-permute-start
  168.7 0.0 copy-done.5
  168.7 0.0 copy-done.2
  168.7 2.7 %multiply_convert_fusion = bf16[768,640]{1,0:T(8,128)(2,1)S(1)} fusion(bf16[2048,1920]{1,0:T(8,128)(2,1)S(1)} %copy-done.2, f32[640]{0:T(1024)S(1)} %copy-done.5, bf16[768,2048]{1,0:T(8,128)(2,1)S(1)} %copy-done, f32[2048]{0:T(1024)S(1)} %copy-done.3, f32[768]{0:T(1024)S(1)} %add_rsqrt_fusion), kind=kOutput, calls=%fused_computation.33 | convolution fusion | flops 2020540416 | bytes 6766592 | tf_op jit(solution)/shard_map/dot_general | solution.py:67
  171.4 2.8 %collective-permute-start.1 = (bf16[2,640]{1,0:T(2,128)(2,1)S(1)}, bf16[2,640]{1,0:T(2,128)(2,1)S(1)}, u32[]{:S(2)}, u32[]{:S(2)}) collective-permute-start(bf16[2,640]{1,0:T(2,128)(2,1)S(1)} %slice.74), channel_id=1, source_target_pairs={{0,8},{8,16},{16,24},{24,32},{32,40},{40,48},{48,56},{56,64},{64,7... | collective-permute-start | bytes 7688 | tf_op jit(solution)/shard_map/ppermute | solution.py:23
  174.2 0.0 collective-permute-done
  174.3 0.2 maximum_convert_fusion
  174.5 0.0 copy-start.6
  174.5 0.0 copy-start.7
  174.5 0.5 collective-permute-done.1
  175.0 0.2 maximum_convert_fusion.1
  175.2 0.0 copy-done.6
  175.2 0.0 copy-done.7
  175.2 5.4 %convolution_convert_fusion = bf16[768,2048]{1,0:T(8,128)(2,1)} fusion(bf16[2048,1920]{1,0:T(8,128)(2,1)S(1)} %copy-done.2, f32[770,640]{1,0:T(8,128)S(1)} %maximum_convert_fusion.1, f32[770,640]{1,0:T(8,128)S(1)} %maximum_convert_fusion, f32[640]{0:T(1024)S(1)} %get-tuple-element.9, f32[640]{0:T(1024)S(1)} %get-tuple-element.10, ...), kind=kOutput, calls=%fused_computation.5 | convolution fusion | flops 2025652224 | bytes 17596416 | tf_op jit(solution)/shard_map/dot_general | solution.py:76
  180.6 0.0 copy-start.1
  180.6 0.0 reduce-scatter.2.cloned.1.call-update
  180.6 49.6 %reduce-scatter.2.cloned.1.call-done = bf16[768,256]{1,0:T(8,128)(2,1)} async-done(((bf16[768,2048]{1,0:T(8,128)(2,1)}), bf16[768,256]{1,0:T(8,128)(2,1)}) %reduce-scatter.2.cloned.1.call-update) | async-done | bytes 393232 | tf_op jit(solution)/shard_map/reduce_scatter | solution.py:77
  230.2 0.0 copy-done.1
  230.2 1.8 multiply_convert_fusion.2
  (3 shorter events, 0.0 us)
Async XLA Ops:
  6.5 155.8 %copy-start = (bf16[768,2048]{1,0:T(8,128)(2,1)S(1)}, bf16[768,2048]{1,0:T(8,128)(2,1)}, u32[]{:S(2)}) copy-start(bf16[768,2048]{1,0:T(8,128)(2,1)} %param.12) | copy-start | bytes 9437188
  6.5 155.8 %copy-start.3 = (f32[2048]{0:T(1024)S(1)}, f32[2048]{0:T(1024)}, u32[]{:S(2)}) copy-start(f32[2048]{0:T(1024)} %param.13) | copy-start | bytes 24580
  6.5 155.8 %copy-start.4 = (f32[640]{0:T(1024)S(1)}, f32[640]{0:T(1024)}, u32[]{:S(2)}) copy-start(f32[640]{0:T(1024)} %param.16) | copy-start | bytes 7684
  6.5 155.8 %all-gather.2.cloned.1.call-start = ((), (), s32[]{:S(2)}) async-start(), calls=%async_computation.1 | async-start | bytes 7987200 | tf_op jit(solution)/shard_map/all_gather | solution.py:12
  10.1 220.2 %reduce-scatter.2.cloned.1.call-start = ((), (), s32[]{:S(2)}) async-start(), calls=%async_computation.2 | async-start | bytes 3538944 | tf_op jit(solution)/shard_map/reduce_scatter | solution.py:77
  13.6 155.1 %copy-start.5 = (f32[640]{0:T(1024)S(1)}, f32[640]{0:T(1024)}, u32[]{:S(2)}) copy-start(f32[640]{0:T(1024)} %param.17) | copy-start | bytes 7684
  162.3 6.4 %copy-start.2 = (bf16[2048,1920]{1,0:T(8,128)(2,1)S(1)}, bf16[2048,1920]{1,0:T(8,128)(2,1)}, u32[]{:S(2)}) copy-start(bf16[2048,1920]{1,0:T(8,128)(2,1)} %all-gather.2.cloned.1.call-done) | copy-start | bytes 23592964
  166.9 7.4 %collective-permute-start = (bf16[2,640]{1,0:T(2,128)(2,1)S(1)}, bf16[2,640]{1,0:T(2,128)(2,1)S(1)}, u32[]{:S(2)}, u32[]{:S(2)}) collective-permute-start(bf16[2,640]{1,0:T(2,128)(2,1)S(1)} %slice.69), channel_id=1, source_target_pairs={{0,8},{8,16},{16,24},{24,32},{32,40},{40,48},{48,56},{56,64},{64,7... | collective-permute-start | bytes 7688 | tf_op jit(solution)/shard_map/ppermute | solution.py:23
  171.4 3.6 %collective-permute-start.1 = (bf16[2,640]{1,0:T(2,128)(2,1)S(1)}, bf16[2,640]{1,0:T(2,128)(2,1)S(1)}, u32[]{:S(2)}, u32[]{:S(2)}) collective-permute-start(bf16[2,640]{1,0:T(2,128)(2,1)S(1)} %slice.74), channel_id=1, source_target_pairs={{0,8},{8,16},{16,24},{24,32},{32,40},{40,48},{48,56},{56,64},{64,7... | collective-permute-start | bytes 7688 | tf_op jit(solution)/shard_map/ppermute | solution.py:23
  174.5 0.7 copy-start.6
  174.5 0.7 copy-start.7
  180.6 49.7 %copy-start.1 = (f32[256]{0:T(256)S(1)}, f32[256]{0:T(256)}, u32[]{:S(2)}) copy-start(f32[256]{0:T(256)} %param.23) | copy-start | bytes 3076
Sparse Core Ops, SparseCore 0:
  10.3 151.9 all-gather.1
  180.7 49.4 reduce-scatter.1
where the time goes:
time: 240 us; the launch traced here: 239 us
  waiting for transfers between devices  199 us (83%)
  between operations  13.5 us (6%)
  matrix products  12.6 us (5%)
  other arithmetic  8.27 us (3%)
  starting transfers between devices  4.64 us (2%)
    all_gather x1, waiting for transfers between devices, gather_turned(): result, at, done = (lax.all_gather(both, axis, axis=0, tiled=True), 0, [])  149 us
    reduce_scatter x1, waiting for transfers between devices, body(): lax.psum_scatter(partial_terms.astype(jnp.bfloat16), 'tp', scatter_dimens...  49.6 us
    dot_general x1, matrix products, body(): jnp.dot(hidden, down_full, preferred_element_type=jnp.float32)  5.38 us
  transfers between devices with their start and end apart: 4, of which 3 were waited for; matrix products, arithmetic and copies ran while one was open for 3% of the time, Pallas kernels for 0%

commit v1 on v0

v1 whole, which is shorter than its diff:
```python
import jax
import jax.numpy as jnp
from jax import lax
from jax.experimental import pallas as pl
from jax.experimental.pallas import tpu as pltpu
from jax.sharding import Mesh, PartitionSpec as P

epsilon = 1e-06
up_lift = 2.0**17
down_lift = 2.0**19
NT = (((1,), (1,)), ((), ()))


def first_half(which, hidden, rows, out):
    out[0] = lax.dot_general(
        hidden[...], rows[0, 0], NT, preferred_element_type=jnp.float32
    ).astype(jnp.bfloat16)


def second_half(which, hidden, rows, received, out):
    product = lax.dot_general(hidden[...], rows[0, 0], NT, preferred_element_type=jnp.float32)
    out[0] = (product + received[0].astype(jnp.float32)).astype(jnp.bfloat16)


def down_part(which, hidden, rows, received=None):
    groups, _, width, depth = rows.shape
    count = hidden.shape[0]
    block = pl.BlockSpec((1, count, width), lambda i, w: (i, 0, 0))
    in_specs = [
        pl.BlockSpec((count, depth), lambda i, w: (0, 0)),
        pl.BlockSpec((1, 1, width, depth), lambda i, w: (i, w[0], 0, 0)),
    ]
    operands = [hidden, rows]
    if received is not None:
        in_specs.append(block)
        operands.append(received)
    return pl.pallas_call(
        first_half if received is None else second_half,
        grid_spec=pltpu.PrefetchScalarGridSpec(
            num_scalar_prefetch=1, grid=(groups,), in_specs=in_specs, out_specs=block
        ),
        out_shape=jax.ShapeDtypeStruct((groups, count, width), jnp.bfloat16),
    )(which, *operands)


def causal_mix(current, previous, kernel, tap_bias):
    row_count = current.shape[0]
    joined = jnp.concatenate([previous, current], axis=0).astype(jnp.float32)
    summed_taps = tap_bias[None, :] + kernel[2][None, :] * joined[2:]
    for back_by in (1, 2):
        summed_taps = (
            summed_taps
            + kernel[2 - back_by][None, :] * joined[2 - back_by : 2 - back_by + row_count]
        )
    return summed_taps


def body(
    tokens,
    norm_gain,
    gate_weight,
    value_weight,
    gate_scale,
    value_scale,
    gate_kernel,
    value_kernel,
    gate_bias,
    value_bias,
    down_weight,
    down_scale,
):
    z_count, y_count = lax.axis_size("z"), lax.axis_size("y")
    x_count, c_count = lax.axis_size("x"), lax.axis_size("c")
    place = lax.axis_index("z") * y_count + lax.axis_index("y")
    core = lax.axis_index("c")
    row_count, width = tokens.shape
    piece, units = gate_weight.shape

    gain = lax.dynamic_slice(norm_gain, (place * piece,), (piece,))[:, None] * up_lift
    shard = jnp.concatenate(
        [gate_weight * gain, value_weight * gain, down_weight.T * down_lift], axis=1
    ).astype(jnp.float16)
    over_z = lax.all_gather(shard, "z", axis=0)
    full = lax.all_gather(over_z, "y", axis=1, tiled=True).reshape(width, 3 * units)

    values = tokens.astype(jnp.float32)
    factor = lax.rsqrt(jnp.mean(values * values, axis=1, keepdims=True) + epsilon) / up_lift
    pre = []
    for at, scale in ((0, gate_scale), (units, value_scale)):
        raw = jnp.dot(
            tokens,
            full[:, at : at + units].astype(jnp.bfloat16),
            preferred_element_type=jnp.float32,
        )
        pre.append((raw * (factor * scale[None, :])).astype(jnp.bfloat16))
    tails = jnp.concatenate([p[row_count - 2 :] for p in pre], axis=1)
    previous = lax.ppermute(
        tails,
        ("z", "y"),
        [(source, source + 1) for source in range(z_count * y_count - 1)],
    )
    gate_conv = causal_mix(pre[0], previous[:, :units], gate_kernel, gate_bias)
    value_conv = causal_mix(pre[1], previous[:, units:], value_kernel, value_bias)
    hidden = (jax.nn.gelu(gate_conv, approximate=True) * value_conv).astype(jnp.bfloat16)

    rows = full[:, 2 * units :].astype(jnp.bfloat16)
    rows = rows.reshape(x_count, c_count, width // (x_count * c_count), units)
    sent = down_part((1 - core).reshape(1), hidden, rows)
    received = lax.ppermute(sent, "c", [(0, 1), (1, 0)])
    paired = down_part(core.reshape(1), hidden, rows, received)
    parts = lax.all_to_all(paired, "x", 0, 0)
    summed = jnp.sum(parts.astype(jnp.float32), axis=0)
    return (summed * (down_scale / down_lift)[None, :]).astype(jnp.bfloat16)


def solution(mesh):
    grid = Mesh(mesh.devices.reshape(16, 4, 4, 2), ("z", "y", "x", "c"))
    fs, tp = ("z", "y"), ("x", "c")
    return jax.shard_map(
        body,
        mesh=grid,
        in_specs=(
            P(fs, None),
            P(),
            P(fs, tp),
            P(fs, tp),
            P(tp),
            P(tp),
            P(None, tp),
            P(None, tp),
            P(tp),
            P(tp),
            P(tp, fs),
            P(tp),
        ),
        out_specs=P(fs, tp),
        check_vma=False,
    )
```

time: 240 us -> 172 us (0.72)
  waiting for transfers between devices: 199 us -> 23.4 us
  blocking collectives: 0 us -> 105 us
  between operations: 13.5 us -> 0.19 us
  starting transfers between devices: 4.64 us -> 16.5 us
  Pallas kernels: 0 us -> 9.92 us
  matrix products: 12.6 us -> 5.29 us
    all_gather x1 -> x0, waiting for transfers between devices: 149 us -> none  [gather_turned(): result, at, done = (lax.all_gather(both, axis, axis=0, tiled=True), 0, [])]
    all_gather x0 -> x2, blocking collectives: none -> 105 us  [the longest x1 61.6 us: body(): lax.all_gather(over_z, 'y', axis=1, tiled=True).reshape(width, 3 * units)]
    reduce_scatter x1 -> x0, waiting for transfers between devices: 49.6 us -> none  [body(): lax.psum_scatter(partial_terms.astype(jnp.bfloat16), 'tp', scatter_dimens...]
    all_to_all x0 -> x1, waiting for transfers between devices: none -> 20.1 us  [body(): parts = lax.all_to_all(paired, 'x', 0, 0)]
    pallas_call x0 -> x2, Pallas kernels: none -> 9.92 us  [down_part(): pl.pallas_call(first_half if received is None else second_half, grid_spec...]
    ppermute x2, starting transfers between devices: 4.6 us -> 12.3 us  [the longest x1 9.38 us: body(): received = lax.ppermute(sent, 'c', [(0, 1), (1, 0)])]
    dot_general x3 -> x2, matrix products: 12.6 us -> 5.29 us  [body(): jnp.dot(tokens, full[:, at:at + units].astype(jnp.bfloat16), preferred_el...]
    all_to_all x0 -> x1, starting transfers between devices: none -> 4.17 us  [body(): parts = lax.all_to_all(paired, 'x', 0, 0)]
  transfers between devices with their start and end apart: 4 -> 3, of which waited for: 3 -> 2; matrix products, arithmetic and copies ran while one was open for 3% -> 1% of each run, Pallas kernels for 0% -> 0%
where the time goes in v1:
time: 172 us; the launch traced here: 171 us
  blocking collectives  105 us (61%)
  waiting for transfers between devices  23.4 us (14%)
  starting transfers between devices  16.5 us (10%)
  Pallas kernels  9.92 us (6%)
  other arithmetic  9.73 us (6%)
  matrix products  5.29 us (3%)
    all_gather x1, blocking collectives, body(): lax.all_gather(over_z, 'y', axis=1, tiled=True).reshape(width, 3 * units)  61.6 us
    all_gather x1, blocking collectives, body(): over_z = lax.all_gather(shard, 'z', axis=0)  43.3 us
    all_to_all x1, waiting for transfers between devices, body(): parts = lax.all_to_all(paired, 'x', 0, 0)  20.1 us
    pallas_call x2, Pallas kernels, down_part(): pl.pallas_call(first_half if received is None else second_half, grid_spec...  9.92 us
    ppermute x1, starting transfers between devices, body(): received = lax.ppermute(sent, 'c', [(0, 1), (1, 0)])  9.38 us
    dot_general x2, matrix products, body(): jnp.dot(tokens, full[:, at:at + units].astype(jnp.bfloat16), preferred_el...  5.29 us
    all_to_all x1, starting transfers between devices, body(): parts = lax.all_to_all(paired, 'x', 0, 0)  4.17 us
  transfers between devices with their start and end apart: 3, of which 2 were waited for; matrix products, arithmetic and copies ran while one was open for 1% of the time, Pallas kernels for 0%

profile of v1, /device:TPU:1, one launch (start us, length us, event | category | flops | bytes accessed | tf_op | source)
XLA Modules:
  0.0 171.4 jit_solution(9326729912771779701)
XLA Ops:
  0.0 0.0 copy-start.2
  0.0 0.0 copy-start.4
  0.0 0.0 copy-start.3
  0.0 2.6 %multiply_reduce_fusion = f32[768]{0:T(1024)S(1)} fusion(bf16[768,2048]{1,0:T(8,128)(2,1)} %param.12), kind=kLoop, calls=%fused_computation | loop fusion | flops 4717824 | bytes 3148800 | tf_op jit(solution)/shard_map/reduce_sum | solution.py:87
  2.6 0.0 copy-done.2
  2.7 0.8 dynamic-slice_multiply_fusion
  3.4 0.0 copy-done.4
  3.4 0.0 copy-done.3
  3.4 0.1 fusion.19
  3.6 43.3 %all-gather.2 = f16[16,32,1920]{2,1,0:T(8,128)(2,1)S(1)} all-gather(f16[1,32,1920]{2,1,0:T(8,128)(2,1)S(1)} %pad_maximum_fusion), channel_id=1, replica_groups=mesh['z'=16,'y'=4,'x'=4,'c'=2] {'z'}, dimensions={0}, use_global_device_ids=true | all-gather | bytes 2088960 | tf_op jit(solution)/shard_map/all_gather | solution.py:83
  46.9 0.0 copy-start
  46.9 0.0 copy-start.10
  46.9 61.6 %all-gather.3 = f16[16,128,1920]{2,1,0:T(8,128)(2,1)S(1)} all-gather(f16[16,32,1920]{2,1,0:T(8,128)(2,1)S(1)} %all-gather.2), channel_id=1, replica_groups=mesh['z'=16,'y'=4,'x'=4,'c'=2] {'y'}, dimensions={1}, use_global_device_ids=true | all-gather | bytes 9830400 | tf_op jit(solution)/shard_map/all_gather | solution.py:84
  108.5 0.0 copy-done
  108.5 0.0 copy-done.10
  108.5 0.0 copy-start.11
  108.5 2.6 %fusion.17 = bf16[768,640]{1,0:T(8,128)(2,1)S(1)} fusion(bf16[768,2048]{1,0:T(8,128)(2,1)S(1)} %copy-done, f16[2048,1920]{1,0:T(8,128)(2,1)S(1)} %bitcast.24, f32[640]{0:T(1024)S(1)} %copy-done.10, f32[768]{0:T(1024)S(1)} %rsqrt_multiply_fusion), kind=kOutput, calls=%fused_computation.30 | convolution fusion | flops 2016051200 | bytes 6758400 | tf_op jit(solution)/shard_map/dot_general | solution.py:90
  111.2 0.0 copy-done.11
  111.2 2.6 %fusion.18 = bf16[768,640]{1,0:T(8,128)(2,1)S(1)} fusion(bf16[768,2048]{1,0:T(8,128)(2,1)S(1)} %copy-done, f16[2048,1920]{1,0:T(8,128)(2,1)S(1)} %bitcast.25, f32[640]{0:T(1024)S(1)} %copy-done.11, f32[768]{0:T(1024)S(1)} %rsqrt_multiply_fusion), kind=kOutput, calls=%fused_computation.32 | convolution fusion | flops 2016051200 | bytes 6758400 | tf_op jit(solution)/shard_map/dot_general | solution.py:90
  113.9 0.0 copy-start.5
  113.9 0.0 copy-start.6
  113.9 2.9 %collective-permute-start = (bf16[2,1280]{1,0:T(2,128)(2,1)S(1)}, bf16[2,1280]{1,0:T(2,128)(2,1)S(1)}, u32[]{:S(2)}, u32[]{:S(2)}) collective-permute-start(bf16[2,1280]{1,0:T(2,128)(2,1)S(1)} %pad_maximum_fusion.1), channel_id=1, source_target_pairs={{0,8},{8,16},{16,24},{24,32},{32,40},{40,48},{48,56},{56,64},{64,7... | collective-permute-start | bytes 15368 | tf_op jit(solution)/shard_map/ppermute | solution.py:97
  116.8 2.0 %slice_convert_fusion = bf16[2048,640]{1,0:T(8,128)(2,1)} fusion(f16[2048,1920]{1,0:T(8,128)(2,1)S(1)} %bitcast.26), kind=kLoop, calls=%fused_computation.3 | loop fusion | flops 1310720 | bytes 5242880 | tf_op jit(solution)/shard_map/convert_element_type | solution.py:106
  118.8 0.0 copy-done.5
  118.8 0.0 copy-done.6
  118.8 0.0 collective-permute-done
  118.9 0.0 copy-start.7
  118.9 0.0 copy-start.8
  118.9 0.4 maximum_convert_fusion
  119.3 0.3 copy-done.7
  119.5 0.0 copy-done.8
  119.6 2.8 %fusion.10.hidden = bf16[768,640]{1,0:T(8,128)(2,1)} fusion(f32[770,640]{1,0:T(8,128)S(1)} %get-tuple-element.16, f32[770,640]{1,0:T(8,128)S(1)} %get-tuple-element.15, f32[640]{0:T(1024)S(1)} %get-tuple-element.9, f32[640]{0:T(1024)S(1)} %get-tuple-element.10, f32[640]{0:T(1024)S(1)} %get-tuple-element.8, f32[640]{0:T(1024)S(1)} %copy-done.7, ...), kind=kLoop, calls=%fused_computation.16 | loop fusion | flops 10813440 | bytes 12800000 | tf_op jit(solution)/shard_map/convert_element_type | solution.py:104
  122.3 4.8 %shard_map.118 = bf16[4,768,256]{2,1,0:T(8,128)(2,1)} custom-call(s32[1]{0:T(128)} %bitcast.9.which, bf16[768,640]{1,0:T(8,128)(2,1)} %fusion.10.hidden, bf16[4,2,256,640]{3,2,1,0:T(8,128)(2,1)} %bitcast.22), custom_call_target="tpu_custom_call" | custom-call | tf_op jit(solution)/shard_map/pallas_call | solution.py:37
  127.2 9.4 %collective-permute-start.1 = (bf16[4,768,256]{2,1,0:T(8,128)(2,1)}, bf16[4,768,256]{2,1,0:T(8,128)(2,1)S(1)}, u32[]{:S(2)}, u32[]{:S(2)}) collective-permute-start(bf16[4,768,256]{2,1,0:T(8,128)(2,1)} %shard_map.118), channel_id=1, source_target_pairs={{0,1},{1,0},{2,3},{3,2},{4,5},{5,4},{6,7},{7,6},{8,9},{9,8},{10,11... | collective-permute-start | bytes 4718600 | tf_op jit(solution)/shard_map/ppermute | solution.py:109
  136.6 3.2 %collective-permute-done.1.received = bf16[4,768,256]{2,1,0:T(8,128)(2,1)S(1)} collective-permute-done((bf16[4,768,256]{2,1,0:T(8,128)(2,1)}, bf16[4,768,256]{2,1,0:T(8,128)(2,1)S(1)}, u32[]{:S(2)}, u32[]{:S(2)}) %collective-permute-start.1) | collective-permute-done | bytes 1572896 | tf_op jit(solution)/shard_map/ppermute | solution.py:109
  139.8 0.0 copy-start.1
  139.8 1.1 copy-done.1
  140.9 5.1 %shard_map.119 = bf16[4,768,256]{2,1,0:T(8,128)(2,1)} custom-call(s32[1]{0:T(128)} %bitcast.which, bf16[768,640]{1,0:T(8,128)(2,1)} %fusion.10.hidden, bf16[4,2,256,640]{3,2,1,0:T(8,128)(2,1)} %bitcast.23, bf16[4,768,256]{2,1,0:T(8,128)(2,1)} %copy-done.1), custom_call_target="tpu_custom_call" | custom-call | tf_op jit(solution)/shard_map/pallas_call | solution.py:37
  146.0 0.0 copy-start.9
  146.0 4.2 %all-to-all-start = ((bf16[4,768,256]{2,1,0:T(8,128)(2,1)}), bf16[4,768,256]{2,1,0:T(8,128)(2,1)S(1)}, u32[]{:S(2)}, u32[]{:S(2)}) async-start(bf16[4,768,256]{2,1,0:T(8,128)(2,1)} %shard_map.119), calls=%async_computation | async-start | bytes 3145728 | tf_op jit(solution)/shard_map/all_to_all | solution.py:111
  150.2 0.0 copy-done.9
  150.2 20.1 %all-to-all-done = bf16[4,768,256]{2,1,0:T(8,128)(2,1)S(1)} async-done(((bf16[4,768,256]{2,1,0:T(8,128)(2,1)}), bf16[4,768,256]{2,1,0:T(8,128)(2,1)S(1)}, u32[]{:S(2)}, u32[]{:S(2)}) %all-to-all-start) | async-done | bytes 1572896 | tf_op jit(solution)/shard_map/all_to_all | solution.py:111
  170.3 0.2 convert_reduce_fusion
  170.6 0.8 multiply_convert_fusion
  (9 shorter events, 0.1 us)
Async XLA Ops:
  0.0 2.6 %copy-start.2 = (f32[640,32]{0,1:T(8,128)S(1)}, f32[640,32]{0,1:T(8,128)}, u32[]{:S(2)}) copy-start(f32[640,32]{0,1:T(8,128)} %param.22) | copy-start | bytes 245764
  0.0 3.4 %copy-start.4 = (f32[32,640]{1,0:T(8,128)S(1)}, f32[32,640]{1,0:T(8,128)}, u32[]{:S(2)}) copy-start(f32[32,640]{1,0:T(8,128)} %param.15) | copy-start | bytes 245764
  0.0 3.4 %copy-start.3 = (f32[32,640]{1,0:T(8,128)S(1)}, f32[32,640]{1,0:T(8,128)}, u32[]{:S(2)}) copy-start(f32[32,640]{1,0:T(8,128)} %param.14) | copy-start | bytes 245764
  46.9 61.6 %copy-start = (bf16[768,2048]{1,0:T(8,128)(2,1)S(1)}, bf16[768,2048]{1,0:T(8,128)(2,1)}, u32[]{:S(2)}) copy-start(bf16[768,2048]{1,0:T(8,128)(2,1)} %param.12) | copy-start | bytes 9437188
  46.9 61.6 %copy-start.10 = (f32[640]{0:T(1024)S(1)}, f32[640]{0:T(1024)}, u32[]{:S(2)}) copy-start(f32[640]{0:T(1024)} %param.17) | copy-start | bytes 7684
  108.5 2.7 %copy-start.11 = (f32[640]{0:T(1024)S(1)}, f32[640]{0:T(1024)}, u32[]{:S(2)}) copy-start(f32[640]{0:T(1024)} %param.16) | copy-start | bytes 7684
  113.9 4.9 %copy-start.5 = (f32[3,640]{1,0:T(4,128)S(1)}, f32[3,640]{1,0:T(4,128)}, u32[]{:S(2)}) copy-start(f32[3,640]{1,0:T(4,128)} %param.19) | copy-start | bytes 23044
  113.9 4.9 %copy-start.6 = (f32[3,640]{1,0:T(4,128)S(1)}, f32[3,640]{1,0:T(4,128)}, u32[]{:S(2)}) copy-start(f32[3,640]{1,0:T(4,128)} %param.18) | copy-start | bytes 23044
  113.9 5.0 %collective-permute-start = (bf16[2,1280]{1,0:T(2,128)(2,1)S(1)}, bf16[2,1280]{1,0:T(2,128)(2,1)S(1)}, u32[]{:S(2)}, u32[]{:S(2)}) collective-permute-start(bf16[2,1280]{1,0:T(2,128)(2,1)S(1)} %pad_maximum_fusion.1), channel_id=1, source_target_pairs={{0,8},{8,16},{16,24},{24,32},{32,40},{40,48},{48,56},{56,64},{64,7... | collective-permute-start | bytes 15368 | tf_op jit(solution)/shard_map/ppermute | solution.py:97
  118.9 0.7 copy-start.7
  118.9 0.7 copy-start.8
  127.2 12.6 %collective-permute-start.1 = (bf16[4,768,256]{2,1,0:T(8,128)(2,1)}, bf16[4,768,256]{2,1,0:T(8,128)(2,1)S(1)}, u32[]{:S(2)}, u32[]{:S(2)}) collective-permute-start(bf16[4,768,256]{2,1,0:T(8,128)(2,1)} %shard_map.118), channel_id=1, source_target_pairs={{0,1},{1,0},{2,3},{3,2},{4,5},{5,4},{6,7},{7,6},{8,9},{9,8},{10,11... | collective-permute-start | bytes 4718600 | tf_op jit(solution)/shard_map/ppermute | solution.py:109
  139.8 1.1 copy-start.1
  146.0 4.2 %copy-start.9 = (f32[256]{0:T(256)S(1)}, f32[256]{0:T(256)}, u32[]{:S(2)}) copy-start(f32[256]{0:T(256)} %param.23) | copy-start | bytes 3076
  146.0 24.3 %all-to-all-start = ((bf16[4,768,256]{2,1,0:T(8,128)(2,1)}), bf16[4,768,256]{2,1,0:T(8,128)(2,1)S(1)}, u32[]{:S(2)}, u32[]{:S(2)}) async-start(bf16[4,768,256]{2,1,0:T(8,128)(2,1)} %shard_map.119), calls=%async_computation | async-start | bytes 3145728 | tf_op jit(solution)/shard_map/all_to_all | solution.py:111

commit v2 on v1

--- a/solution.py
+++ b/solution.py
@@ -1,46 +1,23 @@
 import jax
 import jax.numpy as jnp
 from jax import lax
-from jax.experimental import pallas as pl
-from jax.experimental.pallas import tpu as pltpu
+from jax.experimental.layout import Layout, with_layout_constraint
 from jax.sharding import Mesh, PartitionSpec as P
 
 epsilon = 1e-06
 up_lift = 2.0**17
 down_lift = 2.0**19
-NT = (((1,), (1,)), ((), ()))
 
 
-def first_half(which, hidden, rows, out):
-    out[0] = lax.dot_general(
-        hidden[...], rows[0, 0], NT, preferred_element_type=jnp.float32
-    ).astype(jnp.bfloat16)
-
-
-def second_half(which, hidden, rows, received, out):
-    product = lax.dot_general(hidden[...], rows[0, 0], NT, preferred_element_type=jnp.float32)
-    out[0] = (product + received[0].astype(jnp.float32)).astype(jnp.bfloat16)
-
-
-def down_part(which, hidden, rows, received=None):
-    groups, _, width, depth = rows.shape
-    count = hidden.shape[0]
-    block = pl.BlockSpec((1, count, width), lambda i, w: (i, 0, 0))
-    in_specs = [
-        pl.BlockSpec((count, depth), lambda i, w: (0, 0)),
-        pl.BlockSpec((1, 1, width, depth), lambda i, w: (i, w[0], 0, 0)),
-    ]
-    operands = [hidden, rows]
-    if received is not None:
-        in_specs.append(block)
-        operands.append(received)
-    return pl.pallas_call(
-        first_half if received is None else second_half,
-        grid_spec=pltpu.PrefetchScalarGridSpec(
-            num_scalar_prefetch=1, grid=(groups,), in_specs=in_specs, out_specs=block
-        ),
-        out_shape=jax.ShapeDtypeStruct((groups, count, width), jnp.bfloat16),
-    )(which, *operands)
+def down_half(hidden, rows, core):
+    groups, _, part, total = rows.shape
+    units = hidden.shape[1]
+    mine = lax.dynamic_slice(rows, (0, core, 0, total - units), (groups, 1, part, units))
+    mine = mine.reshape(groups * part, units).astype(jnp.bfloat16)
+    product = lax.dot_general(
+        mine, hidden, (((1,), (1,)), ((), ())), preferred_element_type=jnp.float32
+    )
+    return product.reshape(groups, part, -1)
 
 
 def causal_mix(current, previous, kernel, tap_bias):
@@ -82,6 +59,7 @@
     ).astype(jnp.float16)
     over_z = lax.all_gather(shard, "z", axis=0)
     full = lax.all_gather(over_z, "y", axis=1, tiled=True).reshape(width, 3 * units)
+    tokens, full = lax.optimization_barrier((tokens, full))
 
     values = tokens.astype(jnp.float32)
     factor = lax.rsqrt(jnp.mean(values * values, axis=1, keepdims=True) + epsilon) / up_lift
@@ -102,15 +80,17 @@
     gate_conv = causal_mix(pre[0], previous[:, :units], gate_kernel, gate_bias)
     value_conv = causal_mix(pre[1], previous[:, units:], value_kernel, value_bias)
     hidden = (jax.nn.gelu(gate_conv, approximate=True) * value_conv).astype(jnp.bfloat16)
+    hidden = with_layout_constraint(hidden, Layout(major_to_minor=(0, 1)))
 
-    rows = full[:, 2 * units :].astype(jnp.bfloat16)
-    rows = rows.reshape(x_count, c_count, width // (x_count * c_count), units)
-    sent = down_part((1 - core).reshape(1), hidden, rows)
+    rows = full.reshape(x_count, c_count, width // (x_count * c_count), 3 * units)
+    sent = down_half(hidden, rows, 1 - core).astype(jnp.bfloat16)
     received = lax.ppermute(sent, "c", [(0, 1), (1, 0)])
-    paired = down_part(core.reshape(1), hidden, rows, received)
+    kept = lax.optimization_barrier(down_half(hidden, rows, core))
+    paired = (kept + received.astype(jnp.float32)).astype(jnp.bfloat16)
+    last_scale, paired = lax.optimization_barrier((down_scale / down_lift, paired))
     parts = lax.all_to_all(paired, "x", 0, 0)
-    summed = jnp.sum(parts.astype(jnp.float32), axis=0)
-    return (summed * (down_scale / down_lift)[None, :]).astype(jnp.bfloat16)
+    summed = jnp.sum(parts.astype(jnp.float32), axis=0) * last_scale[:, None]
+    return summed.astype(jnp.bfloat16).T
 
 
 def solution(mesh):

time: 172 us -> 164 us (0.953)
  blocking collectives: 105 us -> 129 us
  waiting for transfers between devices: 23.4 us -> 1.09 us
  Pallas kernels: 9.92 us -> 0 us
  matrix products: 5.29 us -> 12 us
  starting transfers between devices: 16.5 us -> 12.9 us
  other arithmetic: 9.73 us -> 6.59 us
    all_to_all x0 -> x1, blocking collectives: none -> 23.7 us  [body(): parts = lax.all_to_all(paired, 'x', 0, 0)]
    all_to_all x1 -> x0, waiting for transfers between devices: 20.1 us -> none  [body(): parts = lax.all_to_all(paired, 'x', 0, 0)]
    pallas_call x2 -> x0, Pallas kernels: 9.92 us -> none  [down_part(): pl.pallas_call(first_half if received is None else second_half, grid_spec...]
    dot_general x0 -> x2, matrix products: none -> 6.79 us  [down_half(): lax.dot_general(mine, hidden, (((1,), (1,)), ((), ())), preferred_element...]
    all_to_all x1 -> x0, starting transfers between devices: 4.17 us -> none  [body(): parts = lax.all_to_all(paired, 'x', 0, 0)]
    ppermute x1, waiting for transfers between devices: 3.23 us -> 0.42 us  [body(): received = lax.ppermute(sent, 'c', [(0, 1), (1, 0)])]
    convert_element_type x2, other arithmetic: 2.79 us -> 0.56 us  [the longest x1 0.45 us: body(): paired = (kept + received.astype(jnp.float32)).astype(jnp.bfloat16)]
    reduce_sum x1, other arithmetic: 2.61 us -> 0.68 us  [body(): jnp.mean(values * values, axis=1, keepdims=True) + epsilon]
  transfers between devices with their start and end apart: 3 -> 2, of which waited for: 2 -> 2; matrix products, arithmetic and copies ran while one was open for 1% -> 2% of each run, Pallas kernels for 0% -> 0%
where the time goes in v2:
time: 164 us; the launch traced here: 163 us
  blocking collectives  129 us (79%)
  starting transfers between devices  12.9 us (8%)
  matrix products  12 us (7%)
  other arithmetic  6.59 us (4%)
    all_gather x1, blocking collectives, body(): lax.all_gather(over_z, 'y', axis=1, tiled=True).reshape(width, 3 * units)  61.6 us
    all_gather x1, blocking collectives, body(): over_z = lax.all_gather(shard, 'z', axis=0)  43.3 us
    all_to_all x1, blocking collectives, body(): parts = lax.all_to_all(paired, 'x', 0, 0)  23.7 us
    ppermute x1, starting transfers between devices, body(): received = lax.ppermute(sent, 'c', [(0, 1), (1, 0)])  9.96 us
    dot_general x2, matrix products, down_half(): lax.dot_general(mine, hidden, (((1,), (1,)), ((), ())), preferred_element...  6.79 us
    dot_general x2, matrix products, body(): jnp.dot(tokens, full[:, at:at + units].astype(jnp.bfloat16), preferred_el...  5.24 us
  transfers between devices with their start and end apart: 2, of which 2 were waited for; matrix products, arithmetic and copies ran while one was open for 2% of the time, Pallas kernels for 0%

profile of v2, /device:TPU:1, one launch (start us, length us, event | category | flops | bytes accessed | tf_op | source)
XLA Modules:
  0.0 162.7 jit_solution(14825666330794606886)
XLA Ops:
  0.0 0.9 fusion.37
  0.9 0.8 dynamic-slice_multiply_fusion
  1.7 1.0 fusion.35
  2.7 43.3 %all-gather.2 = f16[16,32,1920]{2,1,0:T(8,128)(2,1)S(1)} all-gather(f16[1,32,1920]{2,1,0:T(8,128)(2,1)S(1)} %pad_maximum_fusion), channel_id=1, replica_groups=mesh['z'=16,'y'=4,'x'=4,'c'=2] {'z'}, dimensions={0}, use_global_device_ids=true | all-gather | bytes 2088960 | tf_op jit(solution)/shard_map/all_gather | solution.py:60
  46.0 0.0 copy-start.1
  46.1 61.6 %all-gather.3 = f16[16,128,1920]{2,1,0:T(8,128)(2,1)S(1)} all-gather(f16[16,32,1920]{2,1,0:T(8,128)(2,1)S(1)} %all-gather.2), channel_id=1, replica_groups=mesh['z'=16,'y'=4,'x'=4,'c'=2] {'y'}, dimensions={1}, use_global_device_ids=true | all-gather | bytes 9830400 | tf_op jit(solution)/shard_map/all_gather | solution.py:61
  107.6 0.0 copy-start
  107.6 0.0 copy-start.7
  107.6 0.0 copy-done.1
  107.6 0.7 multiply_reduce_fusion
  108.3 0.0 copy-done.7
  108.4 0.0 copy-start.8
  108.4 2.6 %multiply_convert_fusion = bf16[768,640]{1,0:T(8,128)(2,1)S(1)} fusion(bf16[768,2048]{1,0:T(8,128)(2,1)S(1)} %copy-done.1, f16[2048,1920]{1,0:T(8,128)(2,1)S(1)} %bitcast.35, f32[640]{0:T(1024)S(1)} %copy-done.7, f32[768]{0:T(1024)S(1)} %rsqrt_multiply_fusion), kind=kOutput, calls=%fused_computation.31 | convolution fusion | flops 2016051200 | bytes 6758400 | tf_op jit(solution)/shard_map/dot_general | solution.py:68
  111.0 0.0 copy-done
  111.0 0.0 copy-done.8
  111.0 0.0 copy-start.2
  111.0 0.0 copy-start.3
  111.0 2.6 %multiply_convert_fusion.1 = bf16[768,640]{1,0:T(8,128)(2,1)S(1)} fusion(bf16[768,2048]{1,0:T(8,128)(2,1)S(1)} %copy-done.1, f16[2048,1920]{1,0:T(8,128)(2,1)S(1)} %bitcast.36, f32[640]{0:T(1024)S(1)} %copy-done.8, f32[768]{0:T(1024)S(1)} %rsqrt_multiply_fusion), kind=kOutput, calls=%fused_computation.32 | convolution fusion | flops 2016051200 | bytes 6758400 | tf_op jit(solution)/shard_map/dot_general | solution.py:68
  113.7 2.9 %collective-permute-start = (bf16[2,1280]{1,0:T(2,128)(2,1)S(1)}, bf16[2,1280]{1,0:T(2,128)(2,1)S(1)}, u32[]{:S(2)}, u32[]{:S(2)}) collective-permute-start(bf16[2,1280]{1,0:T(2,128)(2,1)S(1)} %pad_maximum_fusion.1), channel_id=1, source_target_pairs={{0,8},{8,16},{16,24},{24,32},{32,40},{40,48},{48,56},{56,64},{64,7... | collective-permute-start | bytes 15368 | tf_op jit(solution)/shard_map/ppermute | solution.py:75
  116.6 0.0 copy-done.2
  116.6 0.0 copy-done.3
  116.7 0.7 collective-permute-done
  117.4 0.0 copy-start.4
  117.4 0.0 copy-start.5
  117.4 0.4 maximum_convert_fusion
  117.8 0.3 copy-done.4
  118.1 0.0 copy-done.5
  118.1 2.0 %fusion.14 = bf16[768,640]{1,0:T(8,128)(2,1)S(1)} fusion(f32[770,640]{1,0:T(8,128)S(1)} %get-tuple-element.24, f32[770,640]{1,0:T(8,128)S(1)} %get-tuple-element.23, f32[640]{0:T(1024)S(1)} %get-tuple-element.17, f32[640]{0:T(1024)S(1)} %get-tuple-element.18, f32[640]{0:T(1024)S(1)} %get-tuple-element.16, f32[640]{0:T(1024)S(1)} %copy-done.4, ...), kind=kLoop, calls=%fused_computation.18 | loop fusion | flops 10813440 | bytes 12800000 | tf_op jit(solution)/shard_map/convert_element_type | solution.py:82
  120.1 0.0 copy-start.6
  120.1 4.0 %convolution_convert_fusion = bf16[4,256,768]{2,1,0:T(8,128)(2,1)} fusion(f16[4,2,256,1920]{3,2,1,0:T(8,128)(2,1)} %bitcast.37, s32[]{:T(128)S(6)} %select_n.11, bf16[768,640]{1,0:T(8,128)(2,1)S(1)} %fusion.14), kind=kOutput, calls=%fused_computation.33 | convolution fusion | flops 1008074752 | bytes 3866628 | tf_op jit(solution)/shard_map/dot_general | solution.py:17
  124.1 10.0 %collective-permute-start.1 = (bf16[4,256,768]{2,1,0:T(8,128)(2,1)}, bf16[4,256,768]{2,1,0:T(8,128)(2,1)S(1)}, u32[]{:S(2)}, u32[]{:S(2)}) collective-permute-start(bf16[4,256,768]{2,1,0:T(8,128)(2,1)} %convolution_convert_fusion), channel_id=1, source_target_pairs={{0,1},{1,0},{2,3},{3,2},{4,5},{5,4},{6,7},{7,6},{8,9},{9,8},{10,11... | collective-permute-start | bytes 4718600 | tf_op jit(solution)/shard_map/ppermute | solution.py:87
  134.1 0.0 copy-done.6
  134.1 2.8 %fusion.28 = f32[4,256,768]{2,1,0:T(8,128)S(1)} fusion(f16[4,2,256,1920]{3,2,1,0:T(8,128)(2,1)} %bitcast.38, s32[]{:T(128)S(6)} %select_n.10, bf16[768,640]{1,0:T(8,128)(2,1)S(1)} %fusion.14), kind=kOutput, calls=%fused_computation.38 | convolution fusion | flops 1007288320 | bytes 5439492 | tf_op jit(solution)/shard_map/dot_general | solution.py:17
  136.9 0.4 collective-permute-done.1
  137.3 0.4 add_convert_fusion
  137.8 23.7 %all_to_all.5 = bf16[4,256,768]{2,1,0:T(8,128)(2,1)S(1)} all-to-all(bf16[4,256,768]{2,1,0:T(8,128)(2,1)S(1)} %add_convert_fusion), channel_id=1, replica_groups=mesh['z'=16,'y'=4,'x'=4,'c'=2] {'x'}, dimensions={0} | all-to-all | bytes 3145728 | tf_op jit(solution)/shard_map/all_to_all | solution.py:91
  161.4 0.2 convert_reduce_fusion
  161.7 0.1 fusion.34
  161.8 0.9 copy.17
  (8 shorter events, 0.1 us)
Async XLA Ops:
  46.0 61.6 %copy-start.1 = (bf16[768,2048]{1,0:T(8,128)(2,1)S(1)}, bf16[768,2048]{1,0:T(8,128)(2,1)}, u32[]{:S(2)}) copy-start(bf16[768,2048]{1,0:T(8,128)(2,1)} %param.12) | copy-start | bytes 9437188
  107.6 3.4 %copy-start = (f16[16,128,1920]{2,1,0:T(8,128)(2,1)}, f16[16,128,1920]{2,1,0:T(8,128)(2,1)S(1)}, u32[]{:S(2)}) copy-start(f16[16,128,1920]{2,1,0:T(8,128)(2,1)S(1)} %all-gather.3) | copy-start | bytes 23592964
  107.6 0.7 copy-start.7
  108.4 2.7 %copy-start.8 = (f32[640]{0:T(1024)S(1)}, f32[640]{0:T(1024)}, u32[]{:S(2)}) copy-start(f32[640]{0:T(1024)} %param.16) | copy-start | bytes 7684
  111.0 5.6 %copy-start.2 = (f32[3,640]{1,0:T(4,128)S(1)}, f32[3,640]{1,0:T(4,128)}, u32[]{:S(2)}) copy-start(f32[3,640]{1,0:T(4,128)} %param.19) | copy-start | bytes 23044
  111.0 5.6 %copy-start.3 = (f32[3,640]{1,0:T(4,128)S(1)}, f32[3,640]{1,0:T(4,128)}, u32[]{:S(2)}) copy-start(f32[3,640]{1,0:T(4,128)} %param.18) | copy-start | bytes 23044
  113.7 3.7 %collective-permute-start = (bf16[2,1280]{1,0:T(2,128)(2,1)S(1)}, bf16[2,1280]{1,0:T(2,128)(2,1)S(1)}, u32[]{:S(2)}, u32[]{:S(2)}) collective-permute-start(bf16[2,1280]{1,0:T(2,128)(2,1)S(1)} %pad_maximum_fusion.1), channel_id=1, source_target_pairs={{0,8},{8,16},{16,24},{24,32},{32,40},{40,48},{48,56},{56,64},{64,7... | collective-permute-start | bytes 15368 | tf_op jit(solution)/shard_map/ppermute | solution.py:75
  117.4 0.7 copy-start.4
  117.4 0.7 copy-start.5
  120.1 14.0 %copy-start.6 = (f32[256]{0:T(256)S(1)}, f32[256]{0:T(256)}, u32[]{:S(2)}) copy-start(f32[256]{0:T(256)} %param.23) | copy-start | bytes 3076
  124.1 13.2 %collective-permute-start.1 = (bf16[4,256,768]{2,1,0:T(8,128)(2,1)}, bf16[4,256,768]{2,1,0:T(8,128)(2,1)S(1)}, u32[]{:S(2)}, u32[]{:S(2)}) collective-permute-start(bf16[4,256,768]{2,1,0:T(8,128)(2,1)} %convolution_convert_fusion), channel_id=1, source_target_pairs={{0,1},{1,0},{2,3},{3,2},{4,5},{5,4},{6,7},{7,6},{8,9},{9,8},{10,11... | collective-permute-start | bytes 4718600 | tf_op jit(solution)/shard_map/ppermute | solution.py:87

commit v3 on v2

v3 whole, which is shorter than its diff:
```python
import jax
import jax.numpy as jnp
from jax import lax
from jax.experimental import pallas as pl
from jax.experimental.pallas import tpu as pltpu
from jax.sharding import Mesh, PartitionSpec as P

epsilon = 1e-06
up_lift = 2.0**17
down_lift = 2.0**19
halo = 8
lanes = 128
swap = [(0, 1), (1, 0)]
NT = (((1,), (1,)), ((), ()))


def call(kernel, out_shape, limit, operands, scratch=()):
    vmem = pl.BlockSpec(memory_space=pltpu.VMEM)
    scalar = pl.BlockSpec(memory_space=pltpu.SMEM)
    return pl.pallas_call(
        kernel,
        in_specs=[scalar if o.dtype == jnp.int32 else vmem for o in operands],
        out_specs=vmem,
        out_shape=out_shape,
        scratch_shapes=list(scratch),
        compiler_params=pltpu.CompilerParams(vmem_limit_bytes=limit * 2**20),
    )(*operands)


def hidden_kernel(
    side, tokens, before, near, far, scales, taps, biases, out, ordered
):
    row_count, width = tokens.shape
    units = out.shape[1]
    half = width // 2
    full_rows = ordered.shape[0]
    squares = jnp.zeros((full_rows, lanes), jnp.float32)
    for k in range(half // lanes):
        for at, which in ((0, side[0]), (half, 1 - side[0])):
            source = pl.ds(pl.multiple_of((2 * k + which) * lanes, lanes), lanes)
            block = jnp.concatenate(
                [tokens[:, source], before[:, source]], axis=0
            )
            ordered[:, at + k * lanes : at + (k + 1) * lanes] = block
            values = block.astype(jnp.float32)
            squares = squares + values * values
    mean = jnp.sum(squares, axis=1, keepdims=True) / width
    factor = lax.rsqrt(mean + epsilon) / up_lift

    def mixed(kind, at, size):
        cut = slice(kind * units + at, kind * units + at + size)
        raw = jnp.dot(ordered[:, :half], near[:, cut], preferred_element_type=jnp.float32)
        raw = raw + jnp.dot(ordered[:, half:], far[:, cut], preferred_element_type=jnp.float32)
        pre = (raw * (factor * scales[kind : kind + 1, at : at + size])).astype(jnp.bfloat16)
        pre = pre.astype(jnp.float32)
        total = biases[kind : kind + 1, at : at + size]
        for back_by in range(3):
            shifted = pltpu.roll(pre, back_by, 0) if back_by else pre
            row = 3 * kind + 2 - back_by
            total = total + taps[row : row + 1, at : at + size] * shifted[:row_count]
        return total

    for at in range(0, units, 2 * lanes):
        size = min(2 * lanes, units - at)
        gate = mixed(0, at, size)
        value = mixed(1, at, size)
        out[:, at : at + size] = (jax.nn.gelu(gate, approximate=True) * value).astype(jnp.bfloat16)


def hidden_units(side, tokens, before, near, far, scales, taps, biases):
    row_count, width = tokens.shape
    units = scales.shape[1]
    return call(
        hidden_kernel,
        jax.ShapeDtypeStruct((row_count, units), jnp.bfloat16),
        32,
        (side, tokens, before, near, far, scales, taps, biases),
        [pltpu.VMEM((row_count + before.shape[0], width), jnp.bfloat16)],
    )


def down_kernel(places, hidden, near, far, out, rows):
    side, core = places[0], places[1]
    groups = out.shape[0]
    first = pl.ds(pl.multiple_of(side * lanes, lanes), lanes)
    second = pl.ds(pl.multiple_of((1 - side) * lanes, lanes), lanes)
    for x in range(groups):
        rows[x, first] = near[2 * x + core]
        rows[x, second] = far[2 * x + core]
        product = lax.dot_general(
            hidden[...], rows[x], NT, preferred_element_type=jnp.float32
        )
        out[x] = product.astype(out.dtype)


def down_half(side, core, hidden, near, far, dtype):
    groups = near.shape[0] // 2
    row_count, units = hidden.shape
    return call(
        down_kernel,
        jax.ShapeDtypeStruct((groups, row_count, 2 * lanes), dtype),
        16,
        (jnp.stack([side, core]), hidden, near, far),
        [pltpu.VMEM((groups, 2 * lanes, units), jnp.bfloat16)],
    )


def body(
    tokens,
    norm_gain,
    gate_weight,
    value_weight,
    gate_scale,
    value_scale,
    gate_kernel,
    value_kernel,
    gate_bias,
    value_bias,
    down_weight,
    down_scale,
):
    side, core = lax.axis_index("zl"), lax.axis_index("c")
    place = lax.axis_index(("zh", "zl", "y"))
    count = lax.axis_size(("zh", "zl", "y"))
    row_count, width = tokens.shape
    piece, units = gate_weight.shape

    before = lax.ppermute(
        tokens[row_count - halo :],
        ("zh", "zl", "y"),
        [(source, source + 1) for source in range(count - 1)],
    )
    gain = lax.dynamic_slice(norm_gain, (place * piece,), (piece,))[:, None] * up_lift
    shard = jnp.concatenate(
        [gate_weight * gain, value_weight * gain, down_weight.T * down_lift], axis=1
    ).astype(jnp.float16)
    over_z = lax.all_gather(shard, "zh", axis=0)
    partner = lax.ppermute(over_z[:, :, : 2 * units], "zl", swap)
    near = lax.all_gather(over_z, "y", axis=1, tiled=True)
    near_down = near[:, :, 2 * units :].astype(jnp.bfloat16)
    far_down = lax.ppermute(near_down, "zl", swap)
    far = lax.all_gather(partner, "y", axis=1, tiled=True)
    near_up = near[:, :, : 2 * units].astype(jnp.bfloat16).reshape(width // 2, 2 * units)
    far_up = far.astype(jnp.bfloat16).reshape(width // 2, 2 * units)

    before = jnp.concatenate([jnp.zeros_like(before), before], axis=0)
    hidden = hidden_units(
        side.reshape(1),
        tokens,
        before,
        near_up,
        far_up,
        jnp.stack([gate_scale, value_scale]),
        jnp.concatenate([gate_kernel, value_kernel], axis=0),
        jnp.stack([gate_bias, value_bias]),
    )
    sent = down_half(side, 1 - core, hidden, near_down, far_down, jnp.bfloat16)
    received = lax.ppermute(sent, "c", swap)
    kept = down_half(side, core, hidden, near_down, far_down, jnp.float32)
    paired = (kept + received.astype(jnp.float32)).astype(jnp.bfloat16)
    last_scale, paired = lax.optimization_barrier((down_scale / down_lift, paired))
    parts = lax.all_to_all(paired, "x", 0, 0)
    summed = jnp.sum(parts.astype(jnp.float32), axis=0) * last_scale[None, :]
    return summed.astype(jnp.bfloat16)


def solution(mesh):
    grid = Mesh(mesh.devices.reshape(8, 2, 4, 4, 2), ("zh", "zl", "y", "x", "c"))
    fs, tp = ("zh", "zl", "y"), ("x", "c")
    return jax.shard_map(
        body,
        mesh=grid,
        in_specs=(
            P(fs, None),
            P(),
            P(fs, tp),
            P(fs, tp),
            P(tp),
            P(tp),
            P(None, tp),
            P(None, tp),
            P(tp),
            P(tp),
            P(tp, fs),
            P(tp),
        ),
        out_specs=P(fs, tp),
        check_vma=False,
    )
```

time: 164 us -> 152 us (0.927)
  blocking collectives: 129 us -> 108 us
  Pallas kernels: 0 us -> 12.3 us
  matrix products: 12 us -> 0 us
  starting transfers between devices: 12.9 us -> 20.4 us
    all_gather x2 -> x3, blocking collectives: 105 us -> 84.8 us  [the longest x1 35 us: body(): over_z = lax.all_gather(shard, 'zh', axis=0)]
    pallas_call x0 -> x3, Pallas kernels: none -> 12.3 us  [call(): pl.pallas_call(kernel, in_specs=[scalar if o.dtype == jnp.int32 else vmem...]
    dot_general x4 -> x0, matrix products: 12 us -> none  [the longest x2 6.79 us: down_half(): lax.dot_general(mine, hidden, (((1,), (1,)), ((), ())), preferred_element...]
    ppermute x2 -> x4, starting transfers between devices: 12.9 us -> 20.4 us  [the longest x1 10 us: body(): received = lax.ppermute(sent, 'c', swap)]
    convert_element_type x3 -> x4, other arithmetic: 2.51 us -> 3.45 us  [the longest x1 1.97 us: body(): near[:, :, :2 * units].astype(jnp.bfloat16).reshape(width // 2, 2 * units)]
  transfers between devices with their start and end apart: 2 -> 4, of which waited for: 2 -> 1; matrix products, arithmetic and copies ran while one was open for 2% -> 4% of each run, Pallas kernels for 0% -> 7%
where the time goes in v3:
time: 152 us
  blocking collectives  108 us (71%)
  starting transfers between devices  20.4 us (13%)
  Pallas kernels  12.3 us (8%)
  other arithmetic  7.04 us (5%)
  local copies, waits for them, and re-layouts  2.23 us (1%)
    all_gather x1, blocking collectives, body(): over_z = lax.all_gather(shard, 'zh', axis=0)  35 us
    all_gather x1, blocking collectives, body(): near = lax.all_gather(over_z, 'y', axis=1, tiled=True)  29.5 us
    all_to_all x1, blocking collectives, body(): parts = lax.all_to_all(paired, 'x', 0, 0)  23.7 us
    all_gather x1, blocking collectives, body(): far = lax.all_gather(partner, 'y', axis=1, tiled=True)  20.3 us
    pallas_call x3, Pallas kernels, call(): pl.pallas_call(kernel, in_specs=[scalar if o.dtype == jnp.int32 else vmem...  12.3 us
    ppermute x1, starting transfers between devices, body(): received = lax.ppermute(sent, 'c', swap)  10 us
    ppermute x1, starting transfers between devices, body(): lax.ppermute(tokens[row_count - halo:], ('zh', 'zl', 'y'), [(source, sour...  4.01 us
    ppermute x1, starting transfers between devices, body(): far_down = lax.ppermute(near_down, 'zl', swap)  3.32 us
  transfers between devices with their start and end apart: 4, of which 1 were waited for; matrix products, arithmetic and copies ran while one was open for 4% of the time, Pallas kernels for 7%

profile of v3, /device:TPU:1, one launch (start us, length us, event | category | flops | bytes accessed | tf_op | source)
XLA Modules:
  0.0 151.7 jit_solution(7915659127377900800)
XLA Ops:
  0.0 0.8 slice.12
  0.8 4.0 %collective-permute-start = (bf16[8,2048]{1,0:T(8,128)(2,1)S(1)}, bf16[8,2048]{1,0:T(8,128)(2,1)S(1)}, u32[]{:S(2)}, u32[]{:S(2)}) collective-permute-start(bf16[8,2048]{1,0:T(8,128)(2,1)S(1)} %slice.12), channel_id=1, source_target_pairs={{0,8},{8,16},{16,24},{24,32},{32,40},{40,48},{48,56},{56,64},{64,7... | collective-permute-start | bytes 98312 | tf_op jit(solution)/shard_map/ppermute | solution.py:128
  4.8 0.9 fusion.2
  5.7 0.8 dynamic-slice_multiply_fusion
  6.5 1.0 fusion
  7.5 35.0 %all_gather.10 = f16[8,32,1920]{2,1,0:T(8,128)(2,1)S(1)} all-gather(f16[1,32,1920]{2,1,0:T(8,128)(2,1)S(1)} %pad_maximum_fusion), channel_id=1, replica_groups=mesh['zh'=8,'zl'=2,'y'=4,'x'=4,'c'=2] {'zh'}, dimensions={0}, use_global_device_ids=true | all-gather | bytes 1105920 | tf_op jit(solution)/shard_map/all_gather | solution.py:137
  42.5 0.1 slice.17
  42.6 3.1 %collective-permute-start.1 = (f16[8,32,1280]{2,1,0:T(8,128)(2,1)S(1)}, f16[8,32,1280]{2,1,0:T(8,128)(2,1)}, u32[]{:S(2)}, u32[]{:S(2)}) collective-permute-start(f16[8,32,1280]{2,1,0:T(8,128)(2,1)S(1)} %slice.17), channel_id=1, source_target_pairs={{0,32},{32,0},{1,33},{33,1},{2,34},{34,2},{3,35},{35,3},{4,36},{36... | collective-permute-start | bytes 1966088 | tf_op jit(solution)/shard_map/ppermute | solution.py:138
  45.7 29.5 %all-gather.3 = f16[8,128,1920]{2,1,0:T(8,128)(2,1)S(1)} all-gather(f16[8,32,1920]{2,1,0:T(8,128)(2,1)S(1)} %all_gather.10), channel_id=1, replica_groups=mesh['zh'=8,'zl'=2,'y'=4,'x'=4,'c'=2] {'y'}, dimensions={1}, use_global_device_ids=true | all-gather | bytes 4915200 | tf_op jit(solution)/shard_map/all_gather | solution.py:139
  75.2 0.2 slice_convert_fusion.1.near
  75.4 0.0 copy-start.4
  75.4 0.0 copy-start.5
  75.4 0.0 copy-start.6
  75.5 0.0 copy-start.7
  75.5 0.0 copy-start.2
  75.5 0.0 copy-start.3
  75.5 3.3 %collective-permute-start.2 = (bf16[8,128,640]{2,1,0:T(8,128)(2,1)S(1)}, bf16[8,128,640]{2,1,0:T(8,128)(2,1)S(1)}, u32[]{:S(2)}, u32[]{:S(2)}) collective-permute-start(bf16[8,128,640]{2,1,0:T(8,128)(2,1)S(1)} %slice_convert_fusion.1.near), channel_id=1, source_target_pairs={{0,32},{32,0},{1,33},{33,1},{2,34},{34,2},{3,35},{35,3},{4,36},{36... | collective-permute-start | bytes 3932168 | tf_op jit(solution)/shard_map/ppermute | solution.py:141
  78.8 2.0 %slice_convert_fusion = bf16[8,128,1280]{2,1,0:T(8,128)(2,1)} fusion(f16[8,128,1920]{2,1,0:T(8,128)(2,1)S(1)} %all-gather.3), kind=kLoop, calls=%fused_computation.2 | loop fusion | flops 1310720 | bytes 5242880 | tf_op jit(solution)/shard_map/convert_element_type | solution.py:143
  80.8 0.0 copy-done.4
  80.8 0.0 copy-done.5
  80.8 0.0 copy-done.6
  80.8 0.0 copy-done.7
  80.9 0.0 copy-done.2
  80.9 0.0 copy-done.3
  80.9 0.1 pad_add_fusion.1.places
  81.0 0.0 collective-permute-done
  81.0 0.0 collective-permute-done.1
  81.0 0.0 copy-start.1
  81.0 20.3 %all-gather.2 = f16[8,128,1280]{2,1,0:T(8,128)(2,1)S(1)} all-gather(f16[8,32,1280]{2,1,0:T(8,128)(2,1)} %collective-permute-done.1), channel_id=1, replica_groups=mesh['zh'=8,'zl'=2,'y'=4,'x'=4,'c'=2] {'y'}, dimensions={1}, use_global_device_ids=true | all-gather | bytes 3276800 | tf_op jit(solution)/shard_map/all_gather | solution.py:142
  101.4 0.0 copy-start
  101.4 0.4 convert_element_type.30
  101.8 0.0 copy-done.1
  101.8 1.3 copy-done
  103.1 8.3 %shard_map.118.hidden = bf16[768,640]{1,0:T(8,128)(2,1)S(1)} custom-call(s32[1]{0:T(128)} %bitcast.side, bf16[768,2048]{1,0:T(8,128)(2,1)S(1)} %copy-done.1, bf16[16,2048]{1,0:T(8,128)(2,1)S(1)} %concatenate.23.before, bf16[1024,1280]{1,0:T(8,128)(2,1)S(1)} %bitcast.13, bf16[1024,1280]{1,0:T(8,128)(2,1)S(1)} %bitcast.14, ...), custom_call_target="tpu_custom_call" | custom-call | tf_op jit(solution)/shard_map/pallas_call | solution.py:20
  111.4 0.0 copy-start.8
  111.4 0.0 collective-permute-done.2.far
  111.4 2.0 %shard_map.120 = bf16[4,768,256]{2,1,0:T(8,128)(2,1)S(1)} custom-call(s32[2]{0:T(128)S(1)} %pad_add_fusion.1.places, bf16[768,640]{1,0:T(8,128)(2,1)S(1)} %shard_map.118.hidden, bf16[8,128,640]{2,1,0:T(8,128)(2,1)S(1)} %slice_convert_fusion.1.near, bf16[8,128,640]{2,1,0:T(8,128)(2,1)S(1)} %collective-permute-done.2.far), custom_call_target="tpu_custom_call" | custom-call | tf_op jit(solution)/shard_map/pallas_call | solution.py:20
  113.4 10.0 %collective-permute-start.3 = (bf16[4,768,256]{2,1,0:T(8,128)(2,1)S(1)}, bf16[4,768,256]{2,1,0:T(8,128)(2,1)S(1)}, u32[]{:S(2)}, u32[]{:S(2)}) collective-permute-start(bf16[4,768,256]{2,1,0:T(8,128)(2,1)S(1)} %shard_map.120), channel_id=1, source_target_pairs={{0,1},{1,0},{2,3},{3,2},{4,5},{5,4},{6,7},{7,6},{8,9},{9,8},{10,11... | collective-permute-start | bytes 4718600 | tf_op jit(solution)/shard_map/ppermute | solution.py:158
  123.5 0.1 pad_add_fusion.places
  123.6 0.0 copy-done.8
  123.6 2.0 %shard_map.119 = f32[4,768,256]{2,1,0:T(8,128)S(1)} custom-call(s32[2]{0:T(128)S(1)} %pad_add_fusion.places, bf16[768,640]{1,0:T(8,128)(2,1)S(1)} %shard_map.118.hidden, bf16[8,128,640]{2,1,0:T(8,128)(2,1)S(1)} %slice_convert_fusion.1.near, bf16[8,128,640]{2,1,0:T(8,128)(2,1)S(1)} %collective-permute-done.2.far), custom_call_target="tpu_custom_call" | custom-call | tf_op jit(solution)/shard_map/pallas_call | solution.py:20
  125.6 0.9 collective-permute-done.3
  126.5 0.4 add_convert_fusion
  126.9 23.7 %all_to_all.5 = bf16[4,768,256]{2,1,0:T(8,128)(2,1)S(1)} all-to-all(bf16[4,768,256]{2,1,0:T(8,128)(2,1)S(1)} %add_convert_fusion), channel_id=1, replica_groups=mesh['zh'=8,'zl'=2,'y'=4,'x'=4,'c'=2] {'x'}, dimensions={0} | all-to-all | bytes 3145728 | tf_op jit(solution)/shard_map/all_to_all | solution.py:162
  150.6 0.2 convert_reduce_fusion
  150.9 0.8 multiply_convert_fusion
  (9 shorter events, 0.1 us)
Async XLA Ops:
  0.8 80.2 %collective-permute-start = (bf16[8,2048]{1,0:T(8,128)(2,1)S(1)}, bf16[8,2048]{1,0:T(8,128)(2,1)S(1)}, u32[]{:S(2)}, u32[]{:S(2)}) collective-permute-start(bf16[8,2048]{1,0:T(8,128)(2,1)S(1)} %slice.12), channel_id=1, source_target_pairs={{0,8},{8,16},{16,24},{24,32},{32,40},{40,48},{48,56},{56,64},{64,7... | collective-permute-start | bytes 98312 | tf_op jit(solution)/shard_map/ppermute | solution.py:128
  42.6 38.4 %collective-permute-start.1 = (f16[8,32,1280]{2,1,0:T(8,128)(2,1)S(1)}, f16[8,32,1280]{2,1,0:T(8,128)(2,1)}, u32[]{:S(2)}, u32[]{:S(2)}) collective-permute-start(f16[8,32,1280]{2,1,0:T(8,128)(2,1)S(1)} %slice.17), channel_id=1, source_target_pairs={{0,32},{32,0},{1,33},{33,1},{2,34},{34,2},{3,35},{35,3},{4,36},{36... | collective-permute-start | bytes 1966088 | tf_op jit(solution)/shard_map/ppermute | solution.py:138
  75.4 5.4 %copy-start.4 = (f32[640]{0:T(1024)S(1)}, f32[640]{0:T(1024)}, u32[]{:S(2)}) copy-start(f32[640]{0:T(1024)} %param.16) | copy-start | bytes 7684
  75.4 5.4 %copy-start.5 = (f32[640]{0:T(1024)S(1)}, f32[640]{0:T(1024)}, u32[]{:S(2)}) copy-start(f32[640]{0:T(1024)} %param.17) | copy-start | bytes 7684
  75.4 5.4 %copy-start.6 = (f32[640]{0:T(1024)S(1)}, f32[640]{0:T(1024)}, u32[]{:S(2)}) copy-start(f32[640]{0:T(1024)} %param.20) | copy-start | bytes 7684
  75.5 5.4 %copy-start.7 = (f32[640]{0:T(1024)S(1)}, f32[640]{0:T(1024)}, u32[]{:S(2)}) copy-start(f32[640]{0:T(1024)} %param.21) | copy-start | bytes 7684
  75.5 5.4 %copy-start.2 = (f32[3,640]{1,0:T(4,128)S(1)}, f32[3,640]{1,0:T(4,128)}, u32[]{:S(2)}) copy-start(f32[3,640]{1,0:T(4,128)} %param.19) | copy-start | bytes 23044
  75.5 5.4 %copy-start.3 = (f32[3,640]{1,0:T(4,128)S(1)}, f32[3,640]{1,0:T(4,128)}, u32[]{:S(2)}) copy-start(f32[3,640]{1,0:T(4,128)} %param.18) | copy-start | bytes 23044
  75.5 35.9 %collective-permute-start.2 = (bf16[8,128,640]{2,1,0:T(8,128)(2,1)S(1)}, bf16[8,128,640]{2,1,0:T(8,128)(2,1)S(1)}, u32[]{:S(2)}, u32[]{:S(2)}) collective-permute-start(bf16[8,128,640]{2,1,0:T(8,128)(2,1)S(1)} %slice_convert_fusion.1.near), channel_id=1, source_target_pairs={{0,32},{32,0},{1,33},{33,1},{2,34},{34,2},{3,35},{35,3},{4,36},{36... | collective-permute-start | bytes 3932168 | tf_op jit(solution)/shard_map/ppermute | solution.py:141
  81.0 20.8 %copy-start.1 = (bf16[768,2048]{1,0:T(8,128)(2,1)S(1)}, bf16[768,2048]{1,0:T(8,128)(2,1)}, u32[]{:S(2)}) copy-start(bf16[768,2048]{1,0:T(8,128)(2,1)} %tokens.1) | copy-start | bytes 9437188
  101.4 1.7 %copy-start = (bf16[8,128,1280]{2,1,0:T(8,128)(2,1)S(1)}, bf16[8,128,1280]{2,1,0:T(8,128)(2,1)}, u32[]{:S(2)}) copy-start(bf16[8,128,1280]{2,1,0:T(8,128)(2,1)} %slice_convert_fusion) | copy-start | bytes 7864324
  111.4 12.2 %copy-start.8 = (f32[256]{0:T(256)S(1)}, f32[256]{0:T(256)}, u32[]{:S(2)}) copy-start(f32[256]{0:T(256)} %param.23) | copy-start | bytes 3076
  113.4 13.0 %collective-permute-start.3 = (bf16[4,768,256]{2,1,0:T(8,128)(2,1)S(1)}, bf16[4,768,256]{2,1,0:T(8,128)(2,1)S(1)}, u32[]{:S(2)}, u32[]{:S(2)}) collective-permute-start(bf16[4,768,256]{2,1,0:T(8,128)(2,1)S(1)} %shard_map.120), channel_id=1, source_target_pairs={{0,1},{1,0},{2,3},{3,2},{4,5},{5,4},{6,7},{7,6},{8,9},{9,8},{10,11... | collective-permute-start | bytes 4718600 | tf_op jit(solution)/shard_map/ppermute | solution.py:158

commit v4 on v3

--- a/solution.py
+++ b/solution.py
@@ -14,12 +14,16 @@
 NT = (((1,), (1,)), ((), ()))
 
 
-def call(kernel, out_shape, limit, operands, scratch=()):
+def call(kernel, out_shape, limit, operands, scratch=(), anywhere=()):
     vmem = pl.BlockSpec(memory_space=pltpu.VMEM)
     scalar = pl.BlockSpec(memory_space=pltpu.SMEM)
+    remote = pl.BlockSpec(memory_space=pltpu.HBM)
     return pl.pallas_call(
         kernel,
-        in_specs=[scalar if o.dtype == jnp.int32 else vmem for o in operands],
+        in_specs=[
+            remote if i in anywhere else scalar if o.dtype == jnp.int32 else vmem
+            for i, o in enumerate(operands)
+        ],
         out_specs=vmem,
         out_shape=out_shape,
         scratch_shapes=list(scratch),
@@ -28,43 +32,46 @@
 
 
 def hidden_kernel(
-    side, tokens, before, near, far, scales, taps, biases, out, ordered
+    side, tokens, before, near_source, far, scales, taps, biases, out, ordered, near, arrived
 ):
     row_count, width = tokens.shape
     units = out.shape[1]
     half = width // 2
+
+    fetch = pltpu.make_async_copy(near_source, near, arrived)
+    fetch.start()
     full_rows = ordered.shape[0]
     squares = jnp.zeros((full_rows, lanes), jnp.float32)
     for k in range(half // lanes):
         for at, which in ((0, side[0]), (half, 1 - side[0])):
             source = pl.ds(pl.multiple_of((2 * k + which) * lanes, lanes), lanes)
-            block = jnp.concatenate(
-                [tokens[:, source], before[:, source]], axis=0
-            )
+            block = jnp.concatenate([tokens[:, source], before[:, source]], axis=0)
             ordered[:, at + k * lanes : at + (k + 1) * lanes] = block
             values = block.astype(jnp.float32)
             squares = squares + values * values
     mean = jnp.sum(squares, axis=1, keepdims=True) / width
     factor = lax.rsqrt(mean + epsilon) / up_lift
-
-    def mixed(kind, at, size):
-        cut = slice(kind * units + at, kind * units + at + size)
-        raw = jnp.dot(ordered[:, :half], near[:, cut], preferred_element_type=jnp.float32)
-        raw = raw + jnp.dot(ordered[:, half:], far[:, cut], preferred_element_type=jnp.float32)
-        pre = (raw * (factor * scales[kind : kind + 1, at : at + size])).astype(jnp.bfloat16)
-        pre = pre.astype(jnp.float32)
-        total = biases[kind : kind + 1, at : at + size]
-        for back_by in range(3):
-            shifted = pltpu.roll(pre, back_by, 0) if back_by else pre
-            row = 3 * kind + 2 - back_by
-            total = total + taps[row : row + 1, at : at + size] * shifted[:row_count]
-        return total
-
-    for at in range(0, units, 2 * lanes):
-        size = min(2 * lanes, units - at)
-        gate = mixed(0, at, size)
-        value = mixed(1, at, size)
-        out[:, at : at + size] = (jax.nn.gelu(gate, approximate=True) * value).astype(jnp.bfloat16)
+    fetch.wait()
+
+    for at in range(0, units, lanes):
+        gate_cut, value_cut = slice(at, at + lanes), slice(units + at, units + at + lanes)
+
+        def pair(ref):
+            return jnp.concatenate([ref[:, gate_cut], ref[:, value_cut]], axis=1)
+
+        raw = jnp.dot(ordered[:, half:], pair(far), preferred_element_type=jnp.float32)
+        raw = raw + jnp.dot(ordered[:, :half], pair(near), preferred_element_type=jnp.float32)
+        pre = raw * factor
+        weights = taps[:, at : at + lanes] * jnp.concatenate(
+            [jnp.broadcast_to(scales[kind : kind + 1, at : at + lanes], (3, lanes)) for kind in (0, 1)]
+        )
+        both = jnp.concatenate([weights[:3], weights[3:]], axis=1)
+        total = both[0:1] * pre
+        for row in (1, 2):
+            total = pltpu.roll(total, 1, 0) + both[row : row + 1] * pre
+        gate = total[:row_count, :lanes] + biases[0:1, at : at + lanes]
+        value = total[:row_count, lanes:] + biases[1:2, at : at + lanes]
+        out[:, at : at + lanes] = (jax.nn.gelu(gate, approximate=True) * value).astype(jnp.bfloat16)
 
 
 def hidden_units(side, tokens, before, near, far, scales, taps, biases):
@@ -75,7 +82,12 @@
         jax.ShapeDtypeStruct((row_count, units), jnp.bfloat16),
         32,
         (side, tokens, before, near, far, scales, taps, biases),
-        [pltpu.VMEM((row_count + before.shape[0], width), jnp.bfloat16)],
+        [
+            pltpu.VMEM((row_count + before.shape[0], width), jnp.bfloat16),
+            pltpu.VMEM(near.shape, near.dtype),
+            pltpu.SemaphoreType.DMA,
+        ],
+        anywhere=(3,),
     )
 
 

time: 152 us -> 151 us (level)
  transfers between devices with their start and end apart: 4 -> 4, of which waited for: 1 -> 1; matrix products, arithmetic and copies ran while one was open for 4% -> 4% of each run, Pallas kernels for 7% -> 6%
where the time goes in v4:
time: 151 us
  blocking collectives  108 us (72%)
  starting transfers between devices  20.4 us (14%)
  Pallas kernels  11.5 us (8%)
  other arithmetic  7.04 us (5%)
  local copies, waits for them, and re-layouts  2.23 us (1%)
    all_gather x1, blocking collectives, body(): over_z = lax.all_gather(shard, 'zh', axis=0)  35 us
    all_gather x1, blocking collectives, body(): near = lax.all_gather(over_z, 'y', axis=1, tiled=True)  29.5 us
    all_to_all x1, blocking collectives, body(): parts = lax.all_to_all(paired, 'x', 0, 0)  23.7 us
    all_gather x1, blocking collectives, body(): far = lax.all_gather(partner, 'y', axis=1, tiled=True)  20.3 us
    pallas_call x3, Pallas kernels, call(): pl.pallas_call(kernel, in_specs=[remote if i in anywhere else scalar if o...  11.5 us
    ppermute x1, starting transfers between devices, body(): received = lax.ppermute(sent, 'c', swap)  10 us
    ppermute x1, starting transfers between devices, body(): lax.ppermute(tokens[row_count - halo:], ('zh', 'zl', 'y'), [(source, sour...  4.01 us
    ppermute x1, starting transfers between devices, body(): far_down = lax.ppermute(near_down, 'zl', swap)  3.32 us
  transfers between devices with their start and end apart: 4, of which 1 were waited for; matrix products, arithmetic and copies ran while one was open for 4% of the time, Pallas kernels for 6%

profile of v4, /device:TPU:1, one launch (start us, length us, event | category | flops | bytes accessed | tf_op | source)
XLA Modules:
  0.0 150.9 jit_solution(11103168784908931639)
XLA Ops:
  0.0 0.8 slice.12
  0.8 4.0 %collective-permute-start = (bf16[8,2048]{1,0:T(8,128)(2,1)S(1)}, bf16[8,2048]{1,0:T(8,128)(2,1)S(1)}, u32[]{:S(2)}, u32[]{:S(2)}) collective-permute-start(bf16[8,2048]{1,0:T(8,128)(2,1)S(1)} %slice.12), channel_id=1, source_target_pairs={{0,8},{8,16},{16,24},{24,32},{32,40},{40,48},{48,56},{56,64},{64,7... | collective-permute-start | bytes 98312 | tf_op jit(solution)/shard_map/ppermute | solution.py:140
  4.8 0.9 fusion.2
  5.7 0.8 dynamic-slice_multiply_fusion
  6.5 1.0 fusion
  7.5 35.0 %all_gather.10 = f16[8,32,1920]{2,1,0:T(8,128)(2,1)S(1)} all-gather(f16[1,32,1920]{2,1,0:T(8,128)(2,1)S(1)} %pad_maximum_fusion), channel_id=1, replica_groups=mesh['zh'=8,'zl'=2,'y'=4,'x'=4,'c'=2] {'zh'}, dimensions={0}, use_global_device_ids=true | all-gather | bytes 1105920 | tf_op jit(solution)/shard_map/all_gather | solution.py:149
  42.5 0.1 slice.17
  42.6 3.1 %collective-permute-start.1 = (f16[8,32,1280]{2,1,0:T(8,128)(2,1)S(1)}, f16[8,32,1280]{2,1,0:T(8,128)(2,1)}, u32[]{:S(2)}, u32[]{:S(2)}) collective-permute-start(f16[8,32,1280]{2,1,0:T(8,128)(2,1)S(1)} %slice.17), channel_id=1, source_target_pairs={{0,32},{32,0},{1,33},{33,1},{2,34},{34,2},{3,35},{35,3},{4,36},{36... | collective-permute-start | bytes 1966088 | tf_op jit(solution)/shard_map/ppermute | solution.py:150
  45.7 29.5 %all-gather.3 = f16[8,128,1920]{2,1,0:T(8,128)(2,1)S(1)} all-gather(f16[8,32,1920]{2,1,0:T(8,128)(2,1)S(1)} %all_gather.10), channel_id=1, replica_groups=mesh['zh'=8,'zl'=2,'y'=4,'x'=4,'c'=2] {'y'}, dimensions={1}, use_global_device_ids=true | all-gather | bytes 4915200 | tf_op jit(solution)/shard_map/all_gather | solution.py:151
  75.2 0.2 slice_convert_fusion.1.near
  75.4 0.0 copy-start.4
  75.4 0.0 copy-start.5
  75.4 0.0 copy-start.6
  75.5 0.0 copy-start.7
  75.5 0.0 copy-start.2
  75.5 0.0 copy-start.3
  75.5 3.3 %collective-permute-start.2 = (bf16[8,128,640]{2,1,0:T(8,128)(2,1)S(1)}, bf16[8,128,640]{2,1,0:T(8,128)(2,1)S(1)}, u32[]{:S(2)}, u32[]{:S(2)}) collective-permute-start(bf16[8,128,640]{2,1,0:T(8,128)(2,1)S(1)} %slice_convert_fusion.1.near), channel_id=1, source_target_pairs={{0,32},{32,0},{1,33},{33,1},{2,34},{34,2},{3,35},{35,3},{4,36},{36... | collective-permute-start | bytes 3932168 | tf_op jit(solution)/shard_map/ppermute | solution.py:153
  78.8 2.0 %slice_convert_fusion = bf16[8,128,1280]{2,1,0:T(8,128)(2,1)} fusion(f16[8,128,1920]{2,1,0:T(8,128)(2,1)S(1)} %all-gather.3), kind=kLoop, calls=%fused_computation.2 | loop fusion | flops 1310720 | bytes 5242880 | tf_op jit(solution)/shard_map/convert_element_type | solution.py:155
  80.8 0.0 copy-done.4
  80.8 0.0 copy-done.5
  80.8 0.0 copy-done.6
  80.8 0.0 copy-done.7
  80.9 0.0 copy-done.2
  80.9 0.0 copy-done.3
  80.9 0.1 pad_add_fusion.1.places
  81.0 0.0 collective-permute-done
  81.0 0.0 collective-permute-done.1
  81.0 0.0 copy-start.1
  81.0 20.3 %all-gather.2 = f16[8,128,1280]{2,1,0:T(8,128)(2,1)S(1)} all-gather(f16[8,32,1280]{2,1,0:T(8,128)(2,1)} %collective-permute-done.1), channel_id=1, replica_groups=mesh['zh'=8,'zl'=2,'y'=4,'x'=4,'c'=2] {'y'}, dimensions={1}, use_global_device_ids=true | all-gather | bytes 3276800 | tf_op jit(solution)/shard_map/all_gather | solution.py:154
  101.4 0.0 copy-start
  101.4 0.4 convert_element_type.30
  101.8 0.0 copy-done.1
  101.8 1.3 copy-done
  103.1 7.5 %shard_map.118.hidden = bf16[768,640]{1,0:T(8,128)(2,1)S(1)} custom-call(s32[1]{0:T(128)} %bitcast.side, bf16[768,2048]{1,0:T(8,128)(2,1)S(1)} %copy-done.1, bf16[16,2048]{1,0:T(8,128)(2,1)S(1)} %concatenate.23.before, bf16[1024,1280]{1,0:T(8,128)(2,1)S(1)} %bitcast.13, bf16[1024,1280]{1,0:T(8,128)(2,1)S(1)} %bitcast.14, ...), custom_call_target="tpu_custom_call" | custom-call | tf_op jit(solution)/shard_map/pallas_call | solution.py:21
  110.6 0.0 copy-start.8
  110.6 0.0 collective-permute-done.2.far
  110.6 2.0 %shard_map.120 = bf16[4,768,256]{2,1,0:T(8,128)(2,1)S(1)} custom-call(s32[2]{0:T(128)S(1)} %pad_add_fusion.1.places, bf16[768,640]{1,0:T(8,128)(2,1)S(1)} %shard_map.118.hidden, bf16[8,128,640]{2,1,0:T(8,128)(2,1)S(1)} %slice_convert_fusion.1.near, bf16[8,128,640]{2,1,0:T(8,128)(2,1)S(1)} %collective-permute-done.2.far), custom_call_target="tpu_custom_call" | custom-call | tf_op jit(solution)/shard_map/pallas_call | solution.py:21
  112.6 10.0 %collective-permute-start.3 = (bf16[4,768,256]{2,1,0:T(8,128)(2,1)S(1)}, bf16[4,768,256]{2,1,0:T(8,128)(2,1)S(1)}, u32[]{:S(2)}, u32[]{:S(2)}) collective-permute-start(bf16[4,768,256]{2,1,0:T(8,128)(2,1)S(1)} %shard_map.120), channel_id=1, source_target_pairs={{0,1},{1,0},{2,3},{3,2},{4,5},{5,4},{6,7},{7,6},{8,9},{9,8},{10,11... | collective-permute-start | bytes 4718600 | tf_op jit(solution)/shard_map/ppermute | solution.py:170
  122.7 0.1 pad_add_fusion.places
  122.8 0.0 copy-done.8
  122.8 2.0 %shard_map.119 = f32[4,768,256]{2,1,0:T(8,128)S(1)} custom-call(s32[2]{0:T(128)S(1)} %pad_add_fusion.places, bf16[768,640]{1,0:T(8,128)(2,1)S(1)} %shard_map.118.hidden, bf16[8,128,640]{2,1,0:T(8,128)(2,1)S(1)} %slice_convert_fusion.1.near, bf16[8,128,640]{2,1,0:T(8,128)(2,1)S(1)} %collective-permute-done.2.far), custom_call_target="tpu_custom_call" | custom-call | tf_op jit(solution)/shard_map/pallas_call | solution.py:21
  124.8 0.9 collective-permute-done.3
  125.7 0.4 add_convert_fusion
  126.1 23.7 %all_to_all.5 = bf16[4,768,256]{2,1,0:T(8,128)(2,1)S(1)} all-to-all(bf16[4,768,256]{2,1,0:T(8,128)(2,1)S(1)} %add_convert_fusion), channel_id=1, replica_groups=mesh['zh'=8,'zl'=2,'y'=4,'x'=4,'c'=2] {'x'}, dimensions={0} | all-to-all | bytes 3145728 | tf_op jit(solution)/shard_map/all_to_all | solution.py:174
  149.8 0.2 convert_reduce_fusion
  150.1 0.8 multiply_convert_fusion
  (9 shorter events, 0.1 us)
Async XLA Ops:
  0.8 80.2 %collective-permute-start = (bf16[8,2048]{1,0:T(8,128)(2,1)S(1)}, bf16[8,2048]{1,0:T(8,128)(2,1)S(1)}, u32[]{:S(2)}, u32[]{:S(2)}) collective-permute-start(bf16[8,2048]{1,0:T(8,128)(2,1)S(1)} %slice.12), channel_id=1, source_target_pairs={{0,8},{8,16},{16,24},{24,32},{32,40},{40,48},{48,56},{56,64},{64,7... | collective-permute-start | bytes 98312 | tf_op jit(solution)/shard_map/ppermute | solution.py:140
  42.6 38.4 %collective-permute-start.1 = (f16[8,32,1280]{2,1,0:T(8,128)(2,1)S(1)}, f16[8,32,1280]{2,1,0:T(8,128)(2,1)}, u32[]{:S(2)}, u32[]{:S(2)}) collective-permute-start(f16[8,32,1280]{2,1,0:T(8,128)(2,1)S(1)} %slice.17), channel_id=1, source_target_pairs={{0,32},{32,0},{1,33},{33,1},{2,34},{34,2},{3,35},{35,3},{4,36},{36... | collective-permute-start | bytes 1966088 | tf_op jit(solution)/shard_map/ppermute | solution.py:150
  75.4 5.4 %copy-start.4 = (f32[640]{0:T(1024)S(1)}, f32[640]{0:T(1024)}, u32[]{:S(2)}) copy-start(f32[640]{0:T(1024)} %param.16) | copy-start | bytes 7684
  75.4 5.4 %copy-start.5 = (f32[640]{0:T(1024)S(1)}, f32[640]{0:T(1024)}, u32[]{:S(2)}) copy-start(f32[640]{0:T(1024)} %param.17) | copy-start | bytes 7684
  75.4 5.4 %copy-start.6 = (f32[640]{0:T(1024)S(1)}, f32[640]{0:T(1024)}, u32[]{:S(2)}) copy-start(f32[640]{0:T(1024)} %param.20) | copy-start | bytes 7684
  75.5 5.4 %copy-start.7 = (f32[640]{0:T(1024)S(1)}, f32[640]{0:T(1024)}, u32[]{:S(2)}) copy-start(f32[640]{0:T(1024)} %param.21) | copy-start | bytes 7684
  75.5 5.4 %copy-start.2 = (f32[3,640]{1,0:T(4,128)S(1)}, f32[3,640]{1,0:T(4,128)}, u32[]{:S(2)}) copy-start(f32[3,640]{1,0:T(4,128)} %param.19) | copy-start | bytes 23044
  75.5 5.4 %copy-start.3 = (f32[3,640]{1,0:T(4,128)S(1)}, f32[3,640]{1,0:T(4,128)}, u32[]{:S(2)}) copy-start(f32[3,640]{1,0:T(4,128)} %param.18) | copy-start | bytes 23044
  75.5 35.1 %collective-permute-start.2 = (bf16[8,128,640]{2,1,0:T(8,128)(2,1)S(1)}, bf16[8,128,640]{2,1,0:T(8,128)(2,1)S(1)}, u32[]{:S(2)}, u32[]{:S(2)}) collective-permute-start(bf16[8,128,640]{2,1,0:T(8,128)(2,1)S(1)} %slice_convert_fusion.1.near), channel_id=1, source_target_pairs={{0,32},{32,0},{1,33},{33,1},{2,34},{34,2},{3,35},{35,3},{4,36},{36... | collective-permute-start | bytes 3932168 | tf_op jit(solution)/shard_map/ppermute | solution.py:153
  81.0 20.8 %copy-start.1 = (bf16[768,2048]{1,0:T(8,128)(2,1)S(1)}, bf16[768,2048]{1,0:T(8,128)(2,1)}, u32[]{:S(2)}) copy-start(bf16[768,2048]{1,0:T(8,128)(2,1)} %tokens.1) | copy-start | bytes 9437188
  101.4 1.7 %copy-start = (bf16[8,128,1280]{2,1,0:T(8,128)(2,1)S(1)}, bf16[8,128,1280]{2,1,0:T(8,128)(2,1)}, u32[]{:S(2)}) copy-start(bf16[8,128,1280]{2,1,0:T(8,128)(2,1)} %slice_convert_fusion) | copy-start | bytes 7864324
  110.6 12.2 %copy-start.8 = (f32[256]{0:T(256)S(1)}, f32[256]{0:T(256)}, u32[]{:S(2)}) copy-start(f32[256]{0:T(256)} %param.23) | copy-start | bytes 3076
  112.6 13.0 %collective-permute-start.3 = (bf16[4,768,256]{2,1,0:T(8,128)(2,1)S(1)}, bf16[4,768,256]{2,1,0:T(8,128)(2,1)S(1)}, u32[]{:S(2)}, u32[]{:S(2)}) collective-permute-start(bf16[4,768,256]{2,1,0:T(8,128)(2,1)S(1)} %shard_map.120), channel_id=1, source_target_pairs={{0,1},{1,0},{2,3},{3,2},{4,5},{5,4},{6,7},{7,6},{8,9},{9,8},{10,11... | collective-permute-start | bytes 4718600 | tf_op jit(solution)/shard_map/ppermute | solution.py:170

commit v5 on v4

--- a/solution.py
+++ b/solution.py
@@ -32,13 +32,25 @@
 
 
 def hidden_kernel(
-    side, tokens, before, near_source, far, scales, taps, biases, out, ordered, near, arrived
+    side,
+    tokens,
+    before,
+    near_source,
+    far,
+    scales,
+    taps,
+    biases,
+    gains,
+    out,
+    ordered,
+    near,
+    arrived,
 ):
     row_count, width = tokens.shape
     units = out.shape[1]
     half = width // 2
 
-    fetch = pltpu.make_async_copy(near_source, near, arrived)
+    fetch = pltpu.make_async_copy(near_source.at[:, : near.shape[1]], near, arrived)
     fetch.start()
     full_rows = ordered.shape[0]
     squares = jnp.zeros((full_rows, lanes), jnp.float32)
@@ -46,9 +58,11 @@
         for at, which in ((0, side[0]), (half, 1 - side[0])):
             source = pl.ds(pl.multiple_of((2 * k + which) * lanes, lanes), lanes)
             block = jnp.concatenate([tokens[:, source], before[:, source]], axis=0)
-            ordered[:, at + k * lanes : at + (k + 1) * lanes] = block
             values = block.astype(jnp.float32)
             squares = squares + values * values
+            ordered[:, at + k * lanes : at + (k + 1) * lanes] = (
+                values * gains[:, source]
+            ).astype(jnp.bfloat16)
     mean = jnp.sum(squares, axis=1, keepdims=True) / width
     factor = lax.rsqrt(mean + epsilon) / up_lift
     fetch.wait()
@@ -74,17 +88,17 @@
         out[:, at : at + lanes] = (jax.nn.gelu(gate, approximate=True) * value).astype(jnp.bfloat16)
 
 
-def hidden_units(side, tokens, before, near, far, scales, taps, biases):
+def hidden_units(side, tokens, before, near, far, scales, taps, biases, gains):
     row_count, width = tokens.shape
     units = scales.shape[1]
     return call(
         hidden_kernel,
         jax.ShapeDtypeStruct((row_count, units), jnp.bfloat16),
         32,
-        (side, tokens, before, near, far, scales, taps, biases),
+        (side, tokens, before, near, far, scales, taps, biases, gains),
         [
             pltpu.VMEM((row_count + before.shape[0], width), jnp.bfloat16),
-            pltpu.VMEM(near.shape, near.dtype),
+            pltpu.VMEM(far.shape, far.dtype),
             pltpu.SemaphoreType.DMA,
         ],
         anywhere=(3,),
@@ -97,7 +111,7 @@
     first = pl.ds(pl.multiple_of(side * lanes, lanes), lanes)
     second = pl.ds(pl.multiple_of((1 - side) * lanes, lanes), lanes)
     for x in range(groups):
-        rows[x, first] = near[2 * x + core]
+        rows[x, first] = near[2 * x + core, :, near.shape[2] - rows.shape[2] :]
         rows[x, second] = far[2 * x + core]
         product = lax.dot_general(
             hidden[...], rows[x], NT, preferred_element_type=jnp.float32
@@ -132,7 +146,6 @@
     down_scale,
 ):
     side, core = lax.axis_index("zl"), lax.axis_index("c")
-    place = lax.axis_index(("zh", "zl", "y"))
     count = lax.axis_size(("zh", "zl", "y"))
     row_count, width = tokens.shape
     piece, units = gate_weight.shape
@@ -142,17 +155,16 @@
         ("zh", "zl", "y"),
         [(source, source + 1) for source in range(count - 1)],
     )
-    gain = lax.dynamic_slice(norm_gain, (place * piece,), (piece,))[:, None] * up_lift
     shard = jnp.concatenate(
-        [gate_weight * gain, value_weight * gain, down_weight.T * down_lift], axis=1
+        [gate_weight * up_lift, value_weight * up_lift, down_weight.T * down_lift], axis=1
     ).astype(jnp.float16)
     over_z = lax.all_gather(shard, "zh", axis=0)
     partner = lax.ppermute(over_z[:, :, : 2 * units], "zl", swap)
     near = lax.all_gather(over_z, "y", axis=1, tiled=True)
-    near_down = near[:, :, 2 * units :].astype(jnp.bfloat16)
-    far_down = lax.ppermute(near_down, "zl", swap)
+    near = near.astype(jnp.bfloat16)
+    far_down = lax.ppermute(near[:, :, 2 * units :], "zl", swap)
     far = lax.all_gather(partner, "y", axis=1, tiled=True)
-    near_up = near[:, :, : 2 * units].astype(jnp.bfloat16).reshape(width // 2, 2 * units)
+    near_up = near.reshape(width // 2, 3 * units)
     far_up = far.astype(jnp.bfloat16).reshape(width // 2, 2 * units)
 
     before = jnp.concatenate([jnp.zeros_like(before), before], axis=0)
@@ -165,10 +177,11 @@
         jnp.stack([gate_scale, value_scale]),
         jnp.concatenate([gate_kernel, value_kernel], axis=0),
         jnp.stack([gate_bias, value_bias]),
-    )
-    sent = down_half(side, 1 - core, hidden, near_down, far_down, jnp.bfloat16)
+        norm_gain[None, :],
+    )
+    sent = down_half(side, 1 - core, hidden, near, far_down, jnp.bfloat16)
     received = lax.ppermute(sent, "c", swap)
-    kept = down_half(side, core, hidden, near_down, far_down, jnp.float32)
+    kept = down_half(side, core, hidden, near, far_down, jnp.float32)
     paired = (kept + received.astype(jnp.float32)).astype(jnp.bfloat16)
     last_scale, paired = lax.optimization_barrier((down_scale / down_lift, paired))
     parts = lax.all_to_all(paired, "x", 0, 0)

time: 151 us -> 150 us (level)
  local copies, waits for them, and re-layouts: 2.23 us -> 4.57 us
  other arithmetic: 7.04 us -> 4.79 us
    unnamed x18 -> x22, local copies, waits for them, and re-layouts: 1.34 us -> 3.56 us
    all_gather x1, blocking collectives: 35 us -> 37.1 us  [body(): over_z = lax.all_gather(shard, 'zh', axis=0)]
    all_gather x1, blocking collectives: 20.3 us -> 18.5 us  [body(): far = lax.all_gather(partner, 'y', axis=1, tiled=True)]
  transfers between devices with their start and end apart: 4 -> 4, of which waited for: 1 -> 1; matrix products, arithmetic and copies ran while one was open for 4% -> 2% of each run, Pallas kernels for 6% -> 6%
where the time goes in v5:
time: 150 us
  blocking collectives  107 us (71%)
  starting transfers between devices  20.6 us (14%)
  Pallas kernels  11.7 us (8%)
  other arithmetic  4.79 us (3%)
  local copies, waits for them, and re-layouts  4.57 us (3%)
    all_gather x1, blocking collectives, body(): over_z = lax.all_gather(shard, 'zh', axis=0)  37.1 us
    all_gather x1, blocking collectives, body(): near = lax.all_gather(over_z, 'y', axis=1, tiled=True)  28.3 us
    all_to_all x1, blocking collectives, body(): parts = lax.all_to_all(paired, 'x', 0, 0)  23 us
    all_gather x1, blocking collectives, body(): far = lax.all_gather(partner, 'y', axis=1, tiled=True)  18.5 us
    pallas_call x3, Pallas kernels, call(): pl.pallas_call(kernel, in_specs=[remote if i in anywhere else scalar if o...  11.7 us
    ppermute x1, starting transfers between devices, body(): received = lax.ppermute(sent, 'c', swap)  11.5 us
    ppermute x1, starting transfers between devices, body(): far_down = lax.ppermute(near[:, :, 2 * units:], 'zl', swap)  4.09 us
    unnamed x22, local copies, waits for them, and re-layouts  3.56 us
  transfers between devices with their start and end apart: 4, of which 1 were waited for; matrix products, arithmetic and copies ran while one was open for 2% of the time, Pallas kernels for 6%

profile of v5, /device:TPU:1, one launch (start us, length us, event | category | flops | bytes accessed | tf_op | source)
XLA Modules:
  0.0 149.7 jit_solution(2651577061200436159)
XLA Ops:
  0.0 0.9 fusion.2
  0.9 0.9 fusion
  1.9 37.1 %all_gather.10 = f16[8,32,1920]{2,1,0:T(8,128)(2,1)S(1)} all-gather(f16[1,32,1920]{2,1,0:T(8,128)(2,1)S(1)} %pad_maximum_fusion), channel_id=1, replica_groups=mesh['zh'=8,'zl'=2,'y'=4,'x'=4,'c'=2] {'zh'}, dimensions={0}, use_global_device_ids=true | all-gather | bytes 1105920 | tf_op jit(solution)/shard_map/all_gather | solution.py:161
  39.0 0.1 slice.12
  39.1 2.0 %collective-permute-start.1 = (f16[8,32,1280]{2,1,0:T(8,128)(2,1)S(1)}, f16[8,32,1280]{2,1,0:T(8,128)(2,1)}, u32[]{:S(2)}, u32[]{:S(2)}) collective-permute-start(f16[8,32,1280]{2,1,0:T(8,128)(2,1)S(1)} %slice.12), channel_id=1, source_target_pairs={{0,32},{32,0},{1,33},{33,1},{2,34},{34,2},{3,35},{35,3},{4,36},{36... | collective-permute-start | bytes 1966088 | tf_op jit(solution)/shard_map/ppermute | solution.py:162
  41.1 0.8 slice.9
  41.9 3.0 %collective-permute-start = (bf16[8,2048]{1,0:T(8,128)(2,1)S(1)}, bf16[8,2048]{1,0:T(8,128)(2,1)S(1)}, u32[]{:S(2)}, u32[]{:S(2)}) collective-permute-start(bf16[8,2048]{1,0:T(8,128)(2,1)S(1)} %slice.9), channel_id=1, source_target_pairs={{0,8},{8,16},{16,24},{24,32},{32,40},{40,48},{48,56},{56,64},{64,7... | collective-permute-start | bytes 98312 | tf_op jit(solution)/shard_map/ppermute | solution.py:153
  44.9 28.3 %all-gather.2 = f16[8,128,1920]{2,1,0:T(8,128)(2,1)S(1)} all-gather(f16[8,32,1920]{2,1,0:T(8,128)(2,1)S(1)} %all_gather.10), channel_id=1, replica_groups=mesh['zh'=8,'zl'=2,'y'=4,'x'=4,'c'=2] {'y'}, dimensions={1}, use_global_device_ids=true | all-gather | bytes 4915200 | tf_op jit(solution)/shard_map/all_gather | solution.py:163
  73.1 0.8 convert_element_type.26.near
  73.9 0.0 copy-start.6
  74.0 0.0 copy-start.7
  74.0 0.0 copy-start.8
  74.0 0.0 copy-start.9
  74.0 0.0 copy-start.4
  74.0 0.0 copy-start.5
  74.0 0.1 slice.13
  74.1 0.0 copy-start
  74.1 1.8 %copy-done = bf16[8,128,1920]{2,1,0:T(8,128)(2,1)} copy-done((bf16[8,128,1920]{2,1,0:T(8,128)(2,1)}, bf16[8,128,1920]{2,1,0:T(8,128)(2,1)S(1)}, u32[]{:S(2)}) %copy-start) | copy-done | bytes 3932184
  76.0 4.1 %collective-permute-start.2 = (bf16[8,128,640]{2,1,0:T(8,128)(2,1)S(1)}, bf16[8,128,640]{2,1,0:T(8,128)(2,1)S(1)}, u32[]{:S(2)}, u32[]{:S(2)}) collective-permute-start(bf16[8,128,640]{2,1,0:T(8,128)(2,1)S(1)} %slice.13), channel_id=1, source_target_pairs={{0,32},{32,0},{1,33},{33,1},{2,34},{34,2},{3,35},{35,3},{4,36},{36... | collective-permute-start | bytes 3932168 | tf_op jit(solution)/shard_map/ppermute | solution.py:165
  80.1 0.0 copy-done.6
  80.1 0.0 copy-done.7
  80.1 0.0 copy-done.8
  80.2 0.0 copy-done.9
  80.2 0.0 copy-done.4
  80.2 0.0 copy-done.5
  80.2 0.1 pad_add_fusion.1.places
  80.3 0.0 collective-permute-done
  80.3 0.0 collective-permute-done.1
  80.3 0.0 copy-start.2
  80.4 18.5 %all-gather.3 = f16[8,128,1280]{2,1,0:T(8,128)(2,1)S(1)} all-gather(f16[8,32,1280]{2,1,0:T(8,128)(2,1)} %collective-permute-done.1), channel_id=1, replica_groups=mesh['zh'=8,'zl'=2,'y'=4,'x'=4,'c'=2] {'y'}, dimensions={1}, use_global_device_ids=true | all-gather | bytes 3276800 | tf_op jit(solution)/shard_map/all_gather | solution.py:166
  98.9 0.0 copy-start.1
  98.9 0.4 convert_element_type.27
  99.3 0.0 copy-done.2
  99.3 1.7 %copy-done.1 = bf16[8,128,1920]{2,1,0:T(8,128)(2,1)S(1)} copy-done((bf16[8,128,1920]{2,1,0:T(8,128)(2,1)S(1)}, bf16[8,128,1920]{2,1,0:T(8,128)(2,1)}, u32[]{:S(2)}) %copy-start.1) | copy-done | bytes 3932184
  101.0 0.0 copy-done.3
  101.0 7.7 %shard_map.118.hidden = bf16[768,640]{1,0:T(8,128)(2,1)S(1)} custom-call(s32[1]{0:T(128)} %bitcast.side, bf16[768,2048]{1,0:T(8,128)(2,1)S(1)} %copy-done.2, bf16[16,2048]{1,0:T(8,128)(2,1)S(1)} %concatenate.23.before, bf16[1024,1920]{1,0:T(8,128)(2,1)S(1)} %bitcast.14, bf16[1024,1280]{1,0:T(8,128)(2,1)S(1)} %bitcast.15, ...), custom_call_target="tpu_custom_call" | custom-call | tf_op jit(solution)/shard_map/pallas_call | solution.py:21
  108.7 0.0 copy-start.10
  108.7 0.0 collective-permute-done.2.far
  108.7 2.0 %shard_map.120 = bf16[4,768,256]{2,1,0:T(8,128)(2,1)S(1)} custom-call(s32[2]{0:T(128)S(1)} %pad_add_fusion.1.places, bf16[768,640]{1,0:T(8,128)(2,1)S(1)} %shard_map.118.hidden, bf16[8,128,1920]{2,1,0:T(8,128)(2,1)S(1)} %copy-done.1, bf16[8,128,640]{2,1,0:T(8,128)(2,1)S(1)} %collective-permute-done.2.far), custom_call_target="tpu_custom_call" | custom-call | tf_op jit(solution)/shard_map/pallas_call | solution.py:21
  110.7 11.5 %collective-permute-start.3 = (bf16[4,768,256]{2,1,0:T(8,128)(2,1)S(1)}, bf16[4,768,256]{2,1,0:T(8,128)(2,1)S(1)}, u32[]{:S(2)}, u32[]{:S(2)}) collective-permute-start(bf16[4,768,256]{2,1,0:T(8,128)(2,1)S(1)} %shard_map.120), channel_id=1, source_target_pairs={{0,1},{1,0},{2,3},{3,2},{4,5},{5,4},{6,7},{7,6},{8,9},{9,8},{10,11... | collective-permute-start | bytes 4718600 | tf_op jit(solution)/shard_map/ppermute | solution.py:183
  122.2 0.1 pad_add_fusion.places
  122.3 0.0 copy-done.10
  122.3 2.0 %shard_map.119 = f32[4,768,256]{2,1,0:T(8,128)S(1)} custom-call(s32[2]{0:T(128)S(1)} %pad_add_fusion.places, bf16[768,640]{1,0:T(8,128)(2,1)S(1)} %shard_map.118.hidden, bf16[8,128,1920]{2,1,0:T(8,128)(2,1)S(1)} %copy-done.1, bf16[8,128,640]{2,1,0:T(8,128)(2,1)S(1)} %collective-permute-done.2.far), custom_call_target="tpu_custom_call" | custom-call | tf_op jit(solution)/shard_map/pallas_call | solution.py:21
  124.3 0.9 collective-permute-done.3
  125.2 0.4 add_convert_fusion
  125.6 23.0 %all_to_all.5 = bf16[4,768,256]{2,1,0:T(8,128)(2,1)S(1)} all-to-all(bf16[4,768,256]{2,1,0:T(8,128)(2,1)S(1)} %add_convert_fusion), channel_id=1, replica_groups=mesh['zh'=8,'zl'=2,'y'=4,'x'=4,'c'=2] {'x'}, dimensions={0} | all-to-all | bytes 3145728 | tf_op jit(solution)/shard_map/all_to_all | solution.py:187
  148.7 0.2 convert_reduce_fusion
  148.9 0.8 multiply_convert_fusion
  (10 shorter events, 0.1 us)
Async XLA Ops:
  39.1 41.3 %collective-permute-start.1 = (f16[8,32,1280]{2,1,0:T(8,128)(2,1)S(1)}, f16[8,32,1280]{2,1,0:T(8,128)(2,1)}, u32[]{:S(2)}, u32[]{:S(2)}) collective-permute-start(f16[8,32,1280]{2,1,0:T(8,128)(2,1)S(1)} %slice.12), channel_id=1, source_target_pairs={{0,32},{32,0},{1,33},{33,1},{2,34},{34,2},{3,35},{35,3},{4,36},{36... | collective-permute-start | bytes 1966088 | tf_op jit(solution)/shard_map/ppermute | solution.py:162
  41.9 38.5 %collective-permute-start = (bf16[8,2048]{1,0:T(8,128)(2,1)S(1)}, bf16[8,2048]{1,0:T(8,128)(2,1)S(1)}, u32[]{:S(2)}, u32[]{:S(2)}) collective-permute-start(bf16[8,2048]{1,0:T(8,128)(2,1)S(1)} %slice.9), channel_id=1, source_target_pairs={{0,8},{8,16},{16,24},{24,32},{32,40},{40,48},{48,56},{56,64},{64,7... | collective-permute-start | bytes 98312 | tf_op jit(solution)/shard_map/ppermute | solution.py:153
  73.9 6.2 %copy-start.6 = (f32[640]{0:T(1024)S(1)}, f32[640]{0:T(1024)}, u32[]{:S(2)}) copy-start(f32[640]{0:T(1024)} %param.16) | copy-start | bytes 7684
  74.0 6.2 %copy-start.7 = (f32[640]{0:T(1024)S(1)}, f32[640]{0:T(1024)}, u32[]{:S(2)}) copy-start(f32[640]{0:T(1024)} %param.17) | copy-start | bytes 7684
  74.0 6.2 %copy-start.8 = (f32[640]{0:T(1024)S(1)}, f32[640]{0:T(1024)}, u32[]{:S(2)}) copy-start(f32[640]{0:T(1024)} %param.20) | copy-start | bytes 7684
  74.0 6.2 %copy-start.9 = (f32[640]{0:T(1024)S(1)}, f32[640]{0:T(1024)}, u32[]{:S(2)}) copy-start(f32[640]{0:T(1024)} %param.21) | copy-start | bytes 7684
  74.0 6.2 %copy-start.4 = (f32[3,640]{1,0:T(4,128)S(1)}, f32[3,640]{1,0:T(4,128)}, u32[]{:S(2)}) copy-start(f32[3,640]{1,0:T(4,128)} %param.19) | copy-start | bytes 23044
  74.0 6.2 %copy-start.5 = (f32[3,640]{1,0:T(4,128)S(1)}, f32[3,640]{1,0:T(4,128)}, u32[]{:S(2)}) copy-start(f32[3,640]{1,0:T(4,128)} %param.18) | copy-start | bytes 23044
  74.1 1.9 %copy-start = (bf16[8,128,1920]{2,1,0:T(8,128)(2,1)}, bf16[8,128,1920]{2,1,0:T(8,128)(2,1)S(1)}, u32[]{:S(2)}) copy-start(bf16[8,128,1920]{2,1,0:T(8,128)(2,1)S(1)} %convert_element_type.26.near) | copy-start | bytes 11796484
  76.0 32.7 %collective-permute-start.2 = (bf16[8,128,640]{2,1,0:T(8,128)(2,1)S(1)}, bf16[8,128,640]{2,1,0:T(8,128)(2,1)S(1)}, u32[]{:S(2)}, u32[]{:S(2)}) collective-permute-start(bf16[8,128,640]{2,1,0:T(8,128)(2,1)S(1)} %slice.13), channel_id=1, source_target_pairs={{0,32},{32,0},{1,33},{33,1},{2,34},{34,2},{3,35},{35,3},{4,36},{36... | collective-permute-start | bytes 3932168 | tf_op jit(solution)/shard_map/ppermute | solution.py:165
  80.3 19.0 %copy-start.2 = (bf16[768,2048]{1,0:T(8,128)(2,1)S(1)}, bf16[768,2048]{1,0:T(8,128)(2,1)}, u32[]{:S(2)}) copy-start(bf16[768,2048]{1,0:T(8,128)(2,1)} %tokens.1) | copy-start | bytes 9437188
  98.9 2.1 %copy-start.1 = (bf16[8,128,1920]{2,1,0:T(8,128)(2,1)S(1)}, bf16[8,128,1920]{2,1,0:T(8,128)(2,1)}, u32[]{:S(2)}) copy-start(bf16[8,128,1920]{2,1,0:T(8,128)(2,1)} %copy-done) | copy-start | bytes 11796484
  98.9 2.1 %copy-start.3 = (f32[2048]{0:T(1024)S(1)}, f32[2048]{0:T(1024)}, u32[]{:S(2)}) copy-start(f32[2048]{0:T(1024)} %param.13) | copy-start | bytes 24580
  108.7 13.6 %copy-start.10 = (f32[256]{0:T(256)S(1)}, f32[256]{0:T(256)}, u32[]{:S(2)}) copy-start(f32[256]{0:T(256)} %param.23) | copy-start | bytes 3076
  110.7 14.5 %collective-permute-start.3 = (bf16[4,768,256]{2,1,0:T(8,128)(2,1)S(1)}, bf16[4,768,256]{2,1,0:T(8,128)(2,1)S(1)}, u32[]{:S(2)}, u32[]{:S(2)}) collective-permute-start(bf16[4,768,256]{2,1,0:T(8,128)(2,1)S(1)} %shard_map.120), channel_id=1, source_target_pairs={{0,1},{1,0},{2,3},{3,2},{4,5},{5,4},{6,7},{7,6},{8,9},{9,8},{10,11... | collective-permute-start | bytes 4718600 | tf_op jit(solution)/shard_map/ppermute | solution.py:183

commit v6 on v5

--- a/solution.py
+++ b/solution.py
@@ -35,7 +35,7 @@
     side,
     tokens,
     before,
-    near_source,
+    near,
     far,
     scales,
     taps,
@@ -43,15 +43,11 @@
     gains,
     out,
     ordered,
-    near,
-    arrived,
 ):
     row_count, width = tokens.shape
     units = out.shape[1]
     half = width // 2
 
-    fetch = pltpu.make_async_copy(near_source.at[:, : near.shape[1]], near, arrived)
-    fetch.start()
     full_rows = ordered.shape[0]
     squares = jnp.zeros((full_rows, lanes), jnp.float32)
     for k in range(half // lanes):
@@ -65,7 +61,6 @@
             ).astype(jnp.bfloat16)
     mean = jnp.sum(squares, axis=1, keepdims=True) / width
     factor = lax.rsqrt(mean + epsilon) / up_lift
-    fetch.wait()
 
     for at in range(0, units, lanes):
         gate_cut, value_cut = slice(at, at + lanes), slice(units + at, units + at + lanes)
@@ -98,10 +93,7 @@
         (side, tokens, before, near, far, scales, taps, biases, gains),
         [
             pltpu.VMEM((row_count + before.shape[0], width), jnp.bfloat16),
-            pltpu.VMEM(far.shape, far.dtype),
-            pltpu.SemaphoreType.DMA,
         ],
-        anywhere=(3,),
     )
 
 
@@ -129,6 +121,13 @@
         (jnp.stack([side, core]), hidden, near, far),
         [pltpu.VMEM((groups, 2 * lanes, units), jnp.bfloat16)],
     )
+
+
+def final_kernel(parts, scale, out):
+    summed = parts[0].astype(jnp.float32)
+    for x in range(1, parts.shape[0]):
+        summed = summed + parts[x].astype(jnp.float32)
+    out[...] = (summed * scale[...]).astype(jnp.bfloat16)
 
 
 def body(
@@ -185,8 +184,12 @@
     paired = (kept + received.astype(jnp.float32)).astype(jnp.bfloat16)
     last_scale, paired = lax.optimization_barrier((down_scale / down_lift, paired))
     parts = lax.all_to_all(paired, "x", 0, 0)
-    summed = jnp.sum(parts.astype(jnp.float32), axis=0) * last_scale[None, :]
-    return summed.astype(jnp.bfloat16)
+    return call(
+        final_kernel,
+        jax.ShapeDtypeStruct(parts.shape[1:], jnp.bfloat16),
+        8,
+        (parts, last_scale[None, :]),
+    )
 
 
 def solution(mesh):

time: 150 us -> 150 us (level)
    pallas_call x3 -> x4, Pallas kernels: 11.7 us -> 12.3 us  [call(): pl.pallas_call(kernel, in_specs=[remote if i in anywhere else scalar if o...]
where the time goes in v6:
time: 150 us; the launch traced here: 149 us
  blocking collectives  107 us (71%)
  starting transfers between devices  20.6 us (14%)
  Pallas kernels  12.3 us (8%)
  local copies, waits for them, and re-layouts  4.58 us (3%)
  other arithmetic  3.83 us (3%)
    all_gather x1, blocking collectives, body(): over_z = lax.all_gather(shard, 'zh', axis=0)  37.1 us
    all_gather x1, blocking collectives, body(): near = lax.all_gather(over_z, 'y', axis=1, tiled=True)  28.3 us
    all_to_all x1, blocking collectives, body(): parts = lax.all_to_all(paired, 'x', 0, 0)  23 us
    all_gather x1, blocking collectives, body(): far = lax.all_gather(partner, 'y', axis=1, tiled=True)  18.5 us
    pallas_call x4, Pallas kernels, call(): pl.pallas_call(kernel, in_specs=[remote if i in anywhere else scalar if o...  12.3 us
    ppermute x1, starting transfers between devices, body(): received = lax.ppermute(sent, 'c', swap)  11.5 us
    ppermute x1, starting transfers between devices, body(): far_down = lax.ppermute(near[:, :, 2 * units:], 'zl', swap)  4.09 us
    unnamed x22, local copies, waits for them, and re-layouts  3.57 us
  transfers between devices with their start and end apart: 4, of which 1 were waited for; matrix products, arithmetic and copies ran while one was open for 2% of the time, Pallas kernels for 6%

profile of v6, /device:TPU:1, one launch (start us, length us, event | category | flops | bytes accessed | tf_op | source)
XLA Modules:
  0.0 149.4 jit_solution(2738027228691455498)
XLA Ops:
  0.0 0.9 fusion.2
  0.9 0.9 fusion
  1.9 37.1 %all_gather.10 = f16[8,32,1920]{2,1,0:T(8,128)(2,1)S(1)} all-gather(f16[1,32,1920]{2,1,0:T(8,128)(2,1)S(1)} %pad_maximum_fusion), channel_id=1, replica_groups=mesh['zh'=8,'zl'=2,'y'=4,'x'=4,'c'=2] {'zh'}, dimensions={0}, use_global_device_ids=true | all-gather | bytes 1105920 | tf_op jit(solution)/shard_map/all_gather | solution.py:160
  39.0 0.1 slice.12
  39.1 2.0 %collective-permute-start.1 = (f16[8,32,1280]{2,1,0:T(8,128)(2,1)S(1)}, f16[8,32,1280]{2,1,0:T(8,128)(2,1)}, u32[]{:S(2)}, u32[]{:S(2)}) collective-permute-start(f16[8,32,1280]{2,1,0:T(8,128)(2,1)S(1)} %slice.12), channel_id=1, source_target_pairs={{0,32},{32,0},{1,33},{33,1},{2,34},{34,2},{3,35},{35,3},{4,36},{36... | collective-permute-start | bytes 1966088 | tf_op jit(solution)/shard_map/ppermute | solution.py:161
  41.1 0.8 slice.9
  41.9 3.0 %collective-permute-start = (bf16[8,2048]{1,0:T(8,128)(2,1)S(1)}, bf16[8,2048]{1,0:T(8,128)(2,1)S(1)}, u32[]{:S(2)}, u32[]{:S(2)}) collective-permute-start(bf16[8,2048]{1,0:T(8,128)(2,1)S(1)} %slice.9), channel_id=1, source_target_pairs={{0,8},{8,16},{16,24},{24,32},{32,40},{40,48},{48,56},{56,64},{64,7... | collective-permute-start | bytes 98312 | tf_op jit(solution)/shard_map/ppermute | solution.py:152
  44.9 28.3 %all-gather.2 = f16[8,128,1920]{2,1,0:T(8,128)(2,1)S(1)} all-gather(f16[8,32,1920]{2,1,0:T(8,128)(2,1)S(1)} %all_gather.10), channel_id=1, replica_groups=mesh['zh'=8,'zl'=2,'y'=4,'x'=4,'c'=2] {'y'}, dimensions={1}, use_global_device_ids=true | all-gather | bytes 4915200 | tf_op jit(solution)/shard_map/all_gather | solution.py:162
  73.1 0.8 convert_element_type.20.near
  73.9 0.0 copy-start.6
  74.0 0.0 copy-start.7
  74.0 0.0 copy-start.8
  74.0 0.0 copy-start.9
  74.0 0.0 copy-start.4
  74.0 0.0 copy-start.5
  74.0 0.1 slice.13
  74.1 0.0 copy-start
  74.1 1.9 %copy-done = bf16[8,128,1920]{2,1,0:T(8,128)(2,1)} copy-done((bf16[8,128,1920]{2,1,0:T(8,128)(2,1)}, bf16[8,128,1920]{2,1,0:T(8,128)(2,1)S(1)}, u32[]{:S(2)}) %copy-start) | copy-done | bytes 3932184
  76.0 4.1 %collective-permute-start.2 = (bf16[8,128,640]{2,1,0:T(8,128)(2,1)S(1)}, bf16[8,128,640]{2,1,0:T(8,128)(2,1)S(1)}, u32[]{:S(2)}, u32[]{:S(2)}) collective-permute-start(bf16[8,128,640]{2,1,0:T(8,128)(2,1)S(1)} %slice.13), channel_id=1, source_target_pairs={{0,32},{32,0},{1,33},{33,1},{2,34},{34,2},{3,35},{35,3},{4,36},{36... | collective-permute-start | bytes 3932168 | tf_op jit(solution)/shard_map/ppermute | solution.py:164
  80.1 0.0 copy-done.6
  80.1 0.0 copy-done.7
  80.1 0.0 copy-done.8
  80.2 0.0 copy-done.9
  80.2 0.0 copy-done.4
  80.2 0.0 copy-done.5
  80.2 0.1 pad_add_fusion.1.places
  80.3 0.0 collective-permute-done
  80.3 0.0 collective-permute-done.1
  80.3 0.0 copy-start.2
  80.4 18.5 %all-gather.3 = f16[8,128,1280]{2,1,0:T(8,128)(2,1)S(1)} all-gather(f16[8,32,1280]{2,1,0:T(8,128)(2,1)} %collective-permute-done.1), channel_id=1, replica_groups=mesh['zh'=8,'zl'=2,'y'=4,'x'=4,'c'=2] {'y'}, dimensions={1}, use_global_device_ids=true | all-gather | bytes 3276800 | tf_op jit(solution)/shard_map/all_gather | solution.py:165
  98.9 0.0 copy-start.1
  98.9 0.0 copy-start.3
  98.9 0.4 convert_element_type.21
  99.3 0.0 copy-done.2
  99.3 1.7 %copy-done.1 = bf16[8,128,1920]{2,1,0:T(8,128)(2,1)S(1)} copy-done((bf16[8,128,1920]{2,1,0:T(8,128)(2,1)S(1)}, bf16[8,128,1920]{2,1,0:T(8,128)(2,1)}, u32[]{:S(2)}) %copy-start.1) | copy-done | bytes 3932184
  101.0 0.0 copy-done.3
  101.0 7.3 %shard_map.118.hidden = bf16[768,640]{1,0:T(8,128)(2,1)S(1)} custom-call(s32[1]{0:T(128)} %bitcast.side, bf16[768,2048]{1,0:T(8,128)(2,1)S(1)} %copy-done.2, bf16[16,2048]{1,0:T(8,128)(2,1)S(1)} %concatenate.23.before, bf16[1024,1920]{1,0:T(8,128)(2,1)S(1)} %bitcast.15, bf16[1024,1280]{1,0:T(8,128)(2,1)S(1)} %bitcast.16, ...), custom_call_target="tpu_custom_call" | custom-call | tf_op jit(solution)/shard_map/pallas_call | solution.py:21
  108.3 0.0 copy-start.10
  108.3 0.0 collective-permute-done.2.far
  108.3 2.0 %shard_map.120 = bf16[4,768,256]{2,1,0:T(8,128)(2,1)S(1)} custom-call(s32[2]{0:T(128)S(1)} %pad_add_fusion.1.places, bf16[768,640]{1,0:T(8,128)(2,1)S(1)} %shard_map.118.hidden, bf16[8,128,1920]{2,1,0:T(8,128)(2,1)S(1)} %copy-done.1, bf16[8,128,640]{2,1,0:T(8,128)(2,1)S(1)} %collective-permute-done.2.far), custom_call_target="tpu_custom_call" | custom-call | tf_op jit(solution)/shard_map/pallas_call | solution.py:21
  110.4 11.5 %collective-permute-start.3 = (bf16[4,768,256]{2,1,0:T(8,128)(2,1)S(1)}, bf16[4,768,256]{2,1,0:T(8,128)(2,1)S(1)}, u32[]{:S(2)}, u32[]{:S(2)}) collective-permute-start(bf16[4,768,256]{2,1,0:T(8,128)(2,1)S(1)} %shard_map.120), channel_id=1, source_target_pairs={{0,1},{1,0},{2,3},{3,2},{4,5},{5,4},{6,7},{7,6},{8,9},{9,8},{10,11... | collective-permute-start | bytes 4718600 | tf_op jit(solution)/shard_map/ppermute | solution.py:182
  121.8 0.1 pad_add_fusion.places
  121.9 0.0 copy-done.10
  121.9 2.0 %shard_map.119 = f32[4,768,256]{2,1,0:T(8,128)S(1)} custom-call(s32[2]{0:T(128)S(1)} %pad_add_fusion.places, bf16[768,640]{1,0:T(8,128)(2,1)S(1)} %shard_map.118.hidden, bf16[8,128,1920]{2,1,0:T(8,128)(2,1)S(1)} %copy-done.1, bf16[8,128,640]{2,1,0:T(8,128)(2,1)S(1)} %collective-permute-done.2.far), custom_call_target="tpu_custom_call" | custom-call | tf_op jit(solution)/shard_map/pallas_call | solution.py:21
  123.9 0.9 collective-permute-done.3
  124.8 0.5 add_convert_fusion
  125.4 23.0 %all_to_all.5.parts = bf16[4,768,256]{2,1,0:T(8,128)(2,1)S(1)} all-to-all(bf16[4,768,256]{2,1,0:T(8,128)(2,1)S(1)} %add_convert_fusion), channel_id=1, replica_groups=mesh['zh'=8,'zl'=2,'y'=4,'x'=4,'c'=2] {'x'}, dimensions={0} | all-to-all | bytes 3145728 | tf_op jit(solution)/shard_map/all_to_all | solution.py:186
  148.4 1.0 shard_map.121
  (9 shorter events, 0.1 us)
Async XLA Ops:
  39.1 41.3 %collective-permute-start.1 = (f16[8,32,1280]{2,1,0:T(8,128)(2,1)S(1)}, f16[8,32,1280]{2,1,0:T(8,128)(2,1)}, u32[]{:S(2)}, u32[]{:S(2)}) collective-permute-start(f16[8,32,1280]{2,1,0:T(8,128)(2,1)S(1)} %slice.12), channel_id=1, source_target_pairs={{0,32},{32,0},{1,33},{33,1},{2,34},{34,2},{3,35},{35,3},{4,36},{36... | collective-permute-start | bytes 1966088 | tf_op jit(solution)/shard_map/ppermute | solution.py:161
  41.9 38.5 %collective-permute-start = (bf16[8,2048]{1,0:T(8,128)(2,1)S(1)}, bf16[8,2048]{1,0:T(8,128)(2,1)S(1)}, u32[]{:S(2)}, u32[]{:S(2)}) collective-permute-start(bf16[8,2048]{1,0:T(8,128)(2,1)S(1)} %slice.9), channel_id=1, source_target_pairs={{0,8},{8,16},{16,24},{24,32},{32,40},{40,48},{48,56},{56,64},{64,7... | collective-permute-start | bytes 98312 | tf_op jit(solution)/shard_map/ppermute | solution.py:152
  73.9 6.2 %copy-start.6 = (f32[640]{0:T(1024)S(1)}, f32[640]{0:T(1024)}, u32[]{:S(2)}) copy-start(f32[640]{0:T(1024)} %param.16) | copy-start | bytes 7684
  74.0 6.2 %copy-start.7 = (f32[640]{0:T(1024)S(1)}, f32[640]{0:T(1024)}, u32[]{:S(2)}) copy-start(f32[640]{0:T(1024)} %param.17) | copy-start | bytes 7684
  74.0 6.2 %copy-start.8 = (f32[640]{0:T(1024)S(1)}, f32[640]{0:T(1024)}, u32[]{:S(2)}) copy-start(f32[640]{0:T(1024)} %param.20) | copy-start | bytes 7684
  74.0 6.2 %copy-start.9 = (f32[640]{0:T(1024)S(1)}, f32[640]{0:T(1024)}, u32[]{:S(2)}) copy-start(f32[640]{0:T(1024)} %param.21) | copy-start | bytes 7684
  74.0 6.2 %copy-start.4 = (f32[3,640]{1,0:T(4,128)S(1)}, f32[3,640]{1,0:T(4,128)}, u32[]{:S(2)}) copy-start(f32[3,640]{1,0:T(4,128)} %param.19) | copy-start | bytes 23044
  74.0 6.2 %copy-start.5 = (f32[3,640]{1,0:T(4,128)S(1)}, f32[3,640]{1,0:T(4,128)}, u32[]{:S(2)}) copy-start(f32[3,640]{1,0:T(4,128)} %param.18) | copy-start | bytes 23044
  74.1 1.9 %copy-start = (bf16[8,128,1920]{2,1,0:T(8,128)(2,1)}, bf16[8,128,1920]{2,1,0:T(8,128)(2,1)S(1)}, u32[]{:S(2)}) copy-start(bf16[8,128,1920]{2,1,0:T(8,128)(2,1)S(1)} %convert_element_type.20.near) | copy-start | bytes 11796484
  76.0 32.3 %collective-permute-start.2 = (bf16[8,128,640]{2,1,0:T(8,128)(2,1)S(1)}, bf16[8,128,640]{2,1,0:T(8,128)(2,1)S(1)}, u32[]{:S(2)}, u32[]{:S(2)}) collective-permute-start(bf16[8,128,640]{2,1,0:T(8,128)(2,1)S(1)} %slice.13), channel_id=1, source_target_pairs={{0,32},{32,0},{1,33},{33,1},{2,34},{34,2},{3,35},{35,3},{4,36},{36... | collective-permute-start | bytes 3932168 | tf_op jit(solution)/shard_map/ppermute | solution.py:164
  80.3 19.0 %copy-start.2 = (bf16[768,2048]{1,0:T(8,128)(2,1)S(1)}, bf16[768,2048]{1,0:T(8,128)(2,1)}, u32[]{:S(2)}) copy-start(bf16[768,2048]{1,0:T(8,128)(2,1)} %tokens.1) | copy-start | bytes 9437188
  98.9 2.1 %copy-start.1 = (bf16[8,128,1920]{2,1,0:T(8,128)(2,1)S(1)}, bf16[8,128,1920]{2,1,0:T(8,128)(2,1)}, u32[]{:S(2)}) copy-start(bf16[8,128,1920]{2,1,0:T(8,128)(2,1)} %copy-done) | copy-start | bytes 11796484
  98.9 2.1 %copy-start.3 = (f32[2048]{0:T(1024)S(1)}, f32[2048]{0:T(1024)}, u32[]{:S(2)}) copy-start(f32[2048]{0:T(1024)} %param.13) | copy-start | bytes 24580
  108.3 13.6 %copy-start.10 = (f32[256]{0:T(256)S(1)}, f32[256]{0:T(256)}, u32[]{:S(2)}) copy-start(f32[256]{0:T(256)} %param.23) | copy-start | bytes 3076
  110.4 14.5 %collective-permute-start.3 = (bf16[4,768,256]{2,1,0:T(8,128)(2,1)S(1)}, bf16[4,768,256]{2,1,0:T(8,128)(2,1)S(1)}, u32[]{:S(2)}, u32[]{:S(2)}) collective-permute-start(bf16[4,768,256]{2,1,0:T(8,128)(2,1)S(1)} %shard_map.120), channel_id=1, source_target_pairs={{0,1},{1,0},{2,3},{3,2},{4,5},{5,4},{6,7},{7,6},{8,9},{9,8},{10,11... | collective-permute-start | bytes 4718600 | tf_op jit(solution)/shard_map/ppermute | solution.py:182
